TPU v7x, 512 devices: a whole 4x4x16 slice. The times are simulated.
512 devices in a mesh: ep: 32 (over z, core), tp: 16 (over y, x).
Axes of the slice: x: 4, y: 4, z: 16, core: 2. Of those that a mesh axis runs over, the one named last changes fastest.
Arguments:
- mixer_rows: bfloat16 [8192, 2048], P('ep'), may hold values from -8 to 8
- mixer_gain: float32 [2048], replicated, may hold values from 0.1 to 1.9
- w_query: bfloat16 [2048, 1024], P(None, 'tp'), may hold values from -0.125 to 0.125
- w_key: bfloat16 [2048, 1024], P(None, 'tp'), may hold values from -0.125 to 0.125
- w_value: bfloat16 [2048, 1024], P(None, 'tp'), may hold values from -0.125 to 0.125
- key_shift: float32 [16, 8192], P('tp'), may hold values from -14 to 0
- w_out: bfloat16 [1024, 2048], P(None, 'tp'), may hold values from -0.75 to 0.75
- expert_rows: bfloat16 [4096, 2048], P('ep'), may hold values from -6 to 6
- expert_gain: float32 [2048], replicated, may hold values from 0.1 to 1.9
- routes: int32 [4096, 4], P('ep'), may hold values from 0 to 31, all different within a row; in each aligned block of 128 rows (0 to 127, 128 to 255, ...) at most 32 rows name the same one
- route_weight: float32 [4096, 4], P('ep'), may hold values from 0.05 to 0.6
- w_gate: bfloat16 [32, 2048, 2048], P('ep', None, 'tp'), may hold values from -0.25 to 0.25
- w_up: bfloat16 [32, 2048, 2048], P('ep', None, 'tp'), may hold values from -0.25 to 0.25
- w_down: bfloat16 [32, 2048, 2048], P('ep', None, 'tp'), may hold values from -0.0625 to 0.0625
Outputs:
- mixer_out: bfloat16 [8192, 2048], P('ep', 'tp')
- expert_out: bfloat16 [4096, 2048], P('ep', 'tp')
Inputs may be any that keep to these rules, and one draw needn't show every extreme that they name: `routes`: each row names 4 different experts. In each aligned block of 128 rows no expert is named by more than 32 rows, and in every draw some block names some expert exactly 32 times.
All inputs are finite; a program needn't handle non-finite values.
Results may differ from a plain program's by a relative error of at most 0.0073.
Values may be sent and summed in bfloat16 or wider, within the bound.
A program may use at most 64 MiB of HBM per device.

v0:
```python
import jax
import jax.numpy as jnp
from jax import lax
from jax.sharding import Mesh
from jax.sharding import PartitionSpec as P

EP = ("ep_0", "ep_1")


norm_eps = 1e-06
glu_limit = 7.0
glu_alpha = 1.702


def in_order(blocks, dim):
    shape = list(blocks.shape[1:])
    shape[dim] *= blocks.shape[0]
    return jnp.moveaxis(blocks, 0, dim).reshape(shape)


def all_blocks(shard, axes, turns):
    blocks = shard[None]
    for k in turns:
        blocks = lax.all_gather(blocks, axes[k], axis=0, tiled=True)
    carried = [lax.axis_size(axes[k]) for k in reversed(turns)]
    blocks = blocks.reshape(*carried, *shard.shape)
    turned = sorted(range(len(turns)), key=lambda place: turns[len(turns) - 1 - place])
    return blocks.transpose(*turned, *range(len(turns), blocks.ndim)).reshape(-1, *shard.shape)


def whole_of(shard, axes, turns, dim):
    return in_order(all_blocks(shard, axes, turns), dim)


def copy_for_each(shard, axis):
    devices = lax.axis_size(axis)
    return lax.all_to_all(
        jnp.broadcast_to(shard[None], (devices, *shard.shape)), axis, 0, 0, tiled=True
    )


def gather_directly(shard, axis, dim):
    blocks = copy_for_each(shard, axis)
    return in_order(blocks, dim)


def rms_scale(source, scaling):
    floats = source.astype(jnp.float32)
    inverse = lax.rsqrt(jnp.mean(floats * floats, axis=-1, keepdims=True) + norm_eps)
    return (floats * inverse * scaling).astype(jnp.bfloat16)


def stick_block(queries, packed, shifting, carried, allowed):
    length, head_count, head_width = queries.shape
    key_part = packed[:, : head_count * head_width].reshape(length, head_count, head_width)
    value_part = packed[:, head_count * head_width :].reshape(length, head_count, head_width)
    scores = jnp.einsum("thd,shd->hts", queries, key_part, preferred_element_type=jnp.float32)
    scores = scores * head_width ** (-0.5) + shifting[:, None, :]
    log_stay = jnp.where(allowed, jax.nn.log_sigmoid(-scores), 0.0)
    between = lax.cumsum(log_stay, axis=2, reverse=True) - log_stay
    weights = jnp.where(
        allowed, jnp.exp(jax.nn.log_sigmoid(scores) + between + carried[:, :, None]), 0.0
    )
    contrib = jnp.einsum(
        "hts,shd->thd", weights.astype(jnp.bfloat16), value_part, preferred_element_type=jnp.float32
    )
    return (contrib, carried + jnp.sum(log_stay, axis=2))


def per_device(
    mixer_rows,
    mixer_gain,
    w_query,
    w_key,
    w_value,
    key_shift,
    w_out,
    expert_rows,
    expert_gain,
    routes,
    route_weight,
    w_gate,
    w_up,
    w_down,
):
    length = mixer_rows.shape[0]
    head_count = key_shift.shape[0]
    head_width = w_query.shape[1] // head_count
    normed = rms_scale(mixer_rows, mixer_gain)
    queries = jnp.dot(normed, w_query, preferred_element_type=jnp.float32).astype(jnp.bfloat16)
    key_rows = jnp.dot(normed, w_key, preferred_element_type=jnp.float32).astype(jnp.bfloat16)
    value_rows = jnp.dot(normed, w_value, preferred_element_type=jnp.float32).astype(jnp.bfloat16)
    queries = queries.reshape(length, head_count, head_width)
    packed = jnp.concatenate([key_rows, value_rows], axis=1)
    device = lax.axis_index(EP)
    positions = jnp.arange(length, dtype=jnp.int32)
    strict = (positions[None, :] < positions[:, None])[None]
    own_shift = lax.dynamic_slice_in_dim(key_shift, device * length, length, 1)
    summed, carried = stick_block(
        queries, packed, own_shift, jnp.zeros((head_count, length), jnp.float32), strict
    )
    gathered = whole_of(packed, EP, (0, 1), 0)

    def visiting(offset, status):
        running, carry_now = status
        anchor = device - offset
        block_rows = lax.dynamic_slice_in_dim(gathered, anchor * length, length, 0)
        shifting = lax.dynamic_slice_in_dim(key_shift, anchor * length, length, 1)
        contrib, carry_now = stick_block(queries, block_rows, shifting, carry_now, True)
        return (running + contrib, carry_now)

    summed, carried = lax.fori_loop(1, device + 1, visiting, (summed, carried))
    head_out = summed.reshape(length, head_count * head_width).astype(jnp.bfloat16)
    weight_rows = w_out
    mixer_out = jnp.dot(
        gather_directly(head_out, "tp", 1), weight_rows, preferred_element_type=jnp.float32
    ).astype(jnp.bfloat16)
    tokens_here, top_count = routes.shape
    expert_count = lax.axis_size(EP)
    capacity = 2 * tokens_here * top_count // expert_count
    rows_after_norm = rms_scale(expert_rows, expert_gain)
    chosen = routes.reshape(-1)
    hit_table = (chosen[:, None] == jnp.arange(expert_count, dtype=jnp.int32)[None, :]).astype(
        jnp.int32
    )
    places = jnp.sum((jnp.cumsum(hit_table, axis=0) - 1) * hit_table, axis=1)
    targets = chosen * capacity + places
    assign_ids = jnp.arange(tokens_here * top_count, dtype=jnp.int32) // top_count
    owners = (
        jnp.full((expert_count * capacity,), tokens_here, jnp.int32).at[targets].set(assign_ids)
    )
    padded = jnp.concatenate(
        [rows_after_norm, jnp.zeros((1, rows_after_norm.shape[1]), jnp.bfloat16)], axis=0
    )
    outgoing = padded[owners].reshape(expert_count, capacity, rows_after_norm.shape[1])
    gate_cols = w_gate[0]
    upper_cols = w_up[0]
    down_rows = w_down[0]
    portion_size = capacity // lax.axis_size("tp")
    own_slots = lax.dynamic_slice_in_dim(
        outgoing, lax.axis_index("tp") * portion_size, portion_size, 1
    )
    arrived = lax.all_to_all(own_slots, EP, split_axis=0, concat_axis=0, tiled=True)
    expert_arrived = lax.all_gather(arrived, "tp", axis=1, tiled=True)
    expert_senders, slots_here, feature_count = expert_arrived.shape
    flat_rows = expert_arrived.reshape(expert_senders * slots_here, feature_count)
    gating = jnp.minimum(
        jnp.dot(flat_rows, gate_cols, preferred_element_type=jnp.float32), glu_limit
    )
    linear = jnp.clip(
        jnp.dot(flat_rows, upper_cols, preferred_element_type=jnp.float32), -glu_limit, glu_limit
    )
    hidden = gating * jax.nn.sigmoid(glu_alpha * gating) * (linear + 1.0)
    hidden = hidden.astype(jnp.bfloat16).reshape(expert_senders, slots_here, gate_cols.shape[1])
    senders = hidden.shape[0]
    slot_total = hidden.shape[1]
    portion_units = lax.all_gather(hidden, "tp", axis=2, tiled=True)
    weight_rows = down_rows
    flat_units = portion_units.reshape(senders * slot_total, portion_units.shape[2])
    results = jnp.dot(flat_units, weight_rows, preferred_element_type=jnp.float32)
    leaving = results.astype(jnp.bfloat16).reshape(senders, slot_total, down_rows.shape[1])
    returned = lax.all_to_all(leaving, EP, split_axis=0, concat_axis=0, tiled=True)
    picked = returned.reshape(expert_count * capacity, down_rows.shape[1])[targets].astype(
        jnp.float32
    )
    picked = picked * route_weight.reshape(-1)[:, None]
    expert_out = jnp.sum(picked.reshape(tokens_here, top_count, down_rows.shape[1]), axis=1).astype(
        jnp.bfloat16
    )
    return (mixer_out, expert_out)


def solution(mesh):
    torus = Mesh(mesh.devices.reshape(16, 2, mesh.shape["tp"]), ("ep_0", "ep_1", "tp"))
    return jax.shard_map(
        per_device,
        mesh=torus,
        in_specs=(
            P(EP, None),
            P(),
            P(None, "tp"),
            P(None, "tp"),
            P(None, "tp"),
            P("tp", None),
            P(None, "tp"),
            P(EP, None),
            P(),
            P(EP, None),
            P(EP, None),
            P(EP, None, "tp"),
            P(EP, None, "tp"),
            P(EP, None, "tp"),
        ),
        out_specs=(P(EP, "tp"), P(EP, "tp")),
        check_vma=False,
    )
```

profile of v0, /device:TPU:1, one launch (start us, length us, event | category | flops | bytes accessed | tf_op | source)
XLA Modules:
  0.0 366.4 jit_solution(1222065985565656454)
XLA Ops:
  7.3 1.6 fusion.17
  8.9 1.8 convolution_convert_fusion.2
  10.8 0.5 convolution_convert_fusion.4
  11.3 0.6 pad_maximum_fusion
  12.5 1.2 reduce-window.26
  14.6 2.4 scatter_custom_fusion
  17.1 6.0 %gather_fusion = bf16[1024,2048]{1,0:T(8,128)(2,1)} fusion(bf16[129,2048]{1,0:T(8,128)(2,1)S(1)} %concatenate.7, s32[1024]{0:T(1024)S(1)} %fusion.44), kind=kCustom, calls=%fused_computation | custom fusion | bytes 8392704 | tf_op jit(solution)/shard_map/gather | solution.py:135
  23.1 1.5 constant_dynamic-slice_fusion.1
  24.6 40.3 %all_to_all.15 = bf16[32,2,2048]{2,1,0:T(2,128)(2,1)S(1)} all-to-all(bf16[32,2,2048]{2,1,0:T(2,128)(2,1)S(1)} %constant_dynamic-slice_fusion.1), channel_id=1, replica_groups=mesh['ep_0'=16,'ep_1'=2,'tp'=16] {'ep_0','ep_1'}, dimensions={0} | all-to-all | bytes 524288 | tf_op jit(solution)/shard_map/all_to_all | solution.py:143
  64.9 0.8 copy.66
  65.8 19.3 %all-gather.12.cloned.1.call-done = bf16[4096,128]{0,1:T(8,128)(2,1)} async-done(((bf16[256,128]{0,1:T(8,128)(2,1)}), bf16[4096,128]{0,1:T(8,128)(2,1)}) %all-gather.12.cloned.1.call-update) | async-done | bytes 1048592 | tf_op jit(solution)/shard_map/all_gather | solution.py:24
  85.1 2.5 copy.70
  87.8 72.1 %all-gather.8.cloned.1.call-done = bf16[32,32,2048]{2,0,1:T(8,128)(2,1)} async-done(((bf16[32,2,2048]{2,0,1:T(8,128)(2,1)}), bf16[32,32,2048]{2,0,1:T(8,128)(2,1)}) %all-gather.8.cloned.1.call-update) | async-done | bytes 4194320 | tf_op jit(solution)/shard_map/all_gather | solution.py:144
  159.9 4.5 %copy.67 = bf16[32,32,2048]{2,1,0:T(8,128)(2,1)S(1)} copy(bf16[32,32,2048]{2,0,1:T(8,128)(2,1)} %all-gather.8.cloned.1.call-done) | data formatting | bytes 8388608 | tf_op jit(solution)/shard_map/all_gather | solution.py:144
  164.4 1.3 convolution_minimum_fusion
  165.7 2.0 fusion.22
  167.7 0.7 constant_dynamic-slice_fusion.2
  169.3 2.3 fusion.39
  172.1 12.4 %all-gather.6.cloned.1.call-done = bf16[32,256,128]{1,0,2:T(8,128)(2,1)} async-done(((bf16[16,256,128]{1,0,2:T(8,128)(2,1)}), bf16[32,256,128]{1,0,2:T(8,128)(2,1)}) %all-gather.6.cloned.1.call-update) | async-done | bytes 2097168 | tf_op jit(solution)/shard_map/all_gather | solution.py:24
  184.5 3.5 copy.61
  187.9 4.1 %while.12 = (s32[]{:T(128)}, f32[256,1,64]{0,2,1:T(8,128)S(1)}, f32[1,256]{1,0:T(1,128)S(1)}, s32[]{:T(128)}, s32[]{:T(128)}, /*index=5*/bf16[8192,128]{1,0:T(8,...) while((s32[]{:T(128)}, f32[256,1,64]{0,2,1:T(8,128)S(1)}, ...), condition=%wide.region_8.9_spmd, body=%wide.region_4.8_spmd.sunk | while | flops 27083784 | bytes 2680031 | solution.py:112
  188.0 0.7 constant_dynamic-slice_fusion.4
  189.0 2.3 fusion.78
  192.1 0.8 broadcast_in_dim.17
  192.9 5.5 %all-to-all-start = ((bf16[16,256,64]{1,2,0:T(8,128)(2,1)}), bf16[16,256,64]{1,2,0:T(8,128)(2,1)S(1)}, u32[]{:S(2)}, u32[]{:S(2)}) async-start(bf16[16,256,64]{1,2,0:T(8,128)(2,1)} %broadcast_in_dim.17), calls=%async_computation | async-start | bytes 1048576 | tf_op jit(solution)/shard_map/all_to_all | solution.py:37
  198.4 59.6 %all-gather.10.cloned.1.call-done = bf16[32,32,2048]{2,1,0:T(8,128)(2,1)} async-done(((bf16[32,32,128]{2,1,0:T(8,128)(2,1)}), bf16[32,32,2048]{2,1,0:T(8,128)(2,1)}) %all-gather.10.cloned.1.call-update) | async-done | bytes 4194320 | tf_op jit(solution)/shard_map/all_gather | solution.py:157
  258.0 4.3 %convolution_convert_fusion = bf16[1024,128]{1,0:T(8,128)(2,1)} fusion(bf16[1024,2048]{1,0:T(8,128)(2,1)} %bitcast.152, bf16[1,2048,128]{2,1,0:T(8,128)(2,1)} %param.29), kind=kOutput, calls=%fused_computation.40 | convolution fusion | flops 537001984 | bytes 4980736 | tf_op jit(solution)/shard_map/dot_general | solution.py:160
  262.3 73.1 %all-to-all-start.2 = ((bf16[32,32,128]{2,1,0:T(8,128)(2,1)}), bf16[32,32,128]{2,1,0:T(8,128)(2,1)S(1)}, u32[]{:S(2)}, u32[]{:S(2)}) async-start(bf16[32,32,128]{2,1,0:T(8,128)(2,1)} %bitcast.38), calls=%async_computation.2 | async-start | bytes 524288 | tf_op jit(solution)/shard_map/all_to_all | solution.py:162
  335.5 1.0 convolution_convert_fusion.1
  336.5 21.1 %all-to-all-done.2 = bf16[32,32,128]{2,1,0:T(8,128)(2,1)S(1)} async-done(((bf16[32,32,128]{2,1,0:T(8,128)(2,1)}), bf16[32,32,128]{2,1,0:T(8,128)(2,1)S(1)}, u32[]{:S(2)}, u32[]{:S(2)}) %all-to-all-start.2) | async-done | bytes 262176 | tf_op jit(solution)/shard_map/all_to_all | solution.py:162
  357.6 1.3 gather_fusion.1
  359.0 0.9 fusion.37
  (70 shorter events, 4.4 us)
Async XLA Ops:
  7.2 157.2 %copy-start = (bf16[1,2048,128]{2,1,0:T(8,128)(2,1)S(1)}, bf16[1,2048,128]{2,1,0:T(8,128)(2,1)}, u32[]{:S(2)}) copy-start(bf16[1,2048,128]{2,1,0:T(8,128)(2,1)} %param.27) | copy-start | bytes 1572868
  7.2 3.6 copy-start.2
  7.2 3.6 copy-start.10
  7.2 3.6 copy-start.8
  7.2 77.9 %all-gather.12.cloned.1.call-start = ((), (), s32[]{:S(2)}) async-start(), calls=%async_computation.6 | async-start | bytes 1114112 | tf_op jit(solution)/shard_map/all_gather | solution.py:24
  8.9 3.1 copy-start.5
  8.9 3.4 copy-start.1
  10.8 2.9 copy-start.4
  12.0 147.9 %all-gather.8.cloned.1.call-start = ((), (), s32[]{:S(2)}) async-start(), calls=%async_computation.4 | async-start | bytes 4456448 | tf_op jit(solution)/shard_map/all_gather | solution.py:144
  65.8 118.7 %all-gather.6.cloned.1.call-start = ((), (), s32[]{:S(2)}) async-start(), calls=%async_computation.3 | async-start | bytes 3145728 | tf_op jit(solution)/shard_map/all_gather | solution.py:24
  87.6 170.4 %all-gather.10.cloned.1.call-start = ((), (), s32[]{:S(2)}) async-start(), calls=%async_computation.5 | async-start | bytes 4456448 | tf_op jit(solution)/shard_map/all_gather | solution.py:157
  164.4 1.3 copy-start.7
  165.7 2.7 copy-start.9
  192.9 69.4 %all-to-all-start = ((bf16[16,256,64]{1,2,0:T(8,128)(2,1)}), bf16[16,256,64]{1,2,0:T(8,128)(2,1)S(1)}, u32[]{:S(2)}, u32[]{:S(2)}) async-start(bf16[16,256,64]{1,2,0:T(8,128)(2,1)} %broadcast_in_dim.17), calls=%async_computation | async-start | bytes 1048576 | tf_op jit(solution)/shard_map/all_to_all | solution.py:37
  258.0 77.4 %copy-start.6 = (f32[128,4]{0,1:T(4,128)S(1)}, f32[128,4]{0,1:T(4,128)}, u32[]{:S(2)}) copy-start(f32[128,4]{0,1:T(4,128)} %param.26) | copy-start | bytes 6148
  258.0 77.5 %copy-start.3 = (bf16[1024,128]{1,0:T(8,128)(2,1)S(1)}, bf16[1024,128]{1,0:T(8,128)(2,1)}, u32[]{:S(2)}) copy-start(bf16[1024,128]{1,0:T(8,128)(2,1)} %param.22) | copy-start | bytes 786436
  262.3 95.3 %all-to-all-start.2 = ((bf16[32,32,128]{2,1,0:T(8,128)(2,1)}), bf16[32,32,128]{2,1,0:T(8,128)(2,1)S(1)}, u32[]{:S(2)}, u32[]{:S(2)}) async-start(bf16[32,32,128]{2,1,0:T(8,128)(2,1)} %bitcast.38), calls=%async_computation.2 | async-start | bytes 524288 | tf_op jit(solution)/shard_map/all_to_all | solution.py:162
Sparse Core Ops, SparseCore 0:
  12.1 72.9 all-gather.11
  88.1 71.7 all-gather.7
  162.0 22.4 all-gather.5
  187.3 70.6 all-gather.9
where the time goes:
time: 367 us; the launch traced here: 366 us
  waiting for transfers between devices  185 us (50%)
  starting transfers between devices  79 us (22%)
  blocking collectives  40.3 us (11%)
  local copies, waits for them, and re-layouts  25.8 us (7%)
  between operations  14.1 us (4%)
  matrix products  12.4 us (3%)
  other arithmetic  10.2 us (3%)
    all_to_all x1, starting transfers between devices, per_device(): lax.all_to_all(leaving, EP, split_axis=0, concat_axis=0, tiled=True)  73.1 us
    all_gather x1, waiting for transfers between devices, per_device(): expert_arrived = lax.all_gather(arrived, 'tp', axis=1, tiled=True)  72.1 us
    all_gather x1, waiting for transfers between devices, per_device(): portion_units = lax.all_gather(hidden, 'tp', axis=2, tiled=True)  59.6 us
    all_to_all x1, blocking collectives, per_device(): lax.all_to_all(own_slots, EP, split_axis=0, concat_axis=0, tiled=True)  40.3 us
    all_gather x2, waiting for transfers between devices, all_blocks(): blocks = lax.all_gather(blocks, axes[k], axis=0, tiled=True)  31.7 us
    all_to_all x1, waiting for transfers between devices, per_device(): lax.all_to_all(leaving, EP, split_axis=0, concat_axis=0, tiled=True)  21.1 us
  transfers between devices with their start and end apart: 6, of which 5 were waited for; matrix products, arithmetic and copies ran while one was open for 11% of the time, Pallas kernels for 0%

commit v1 on v0

--- a/solution.py
+++ b/solution.py
@@ -2,6 +2,8 @@
 import jax.numpy as jnp
 from jax import lax
 from jax.sharding import Mesh
+from jax.experimental import pallas as pl
+from jax.experimental.pallas import tpu as pltpu
 from jax.sharding import PartitionSpec as P
 
 EP = ("ep_0", "ep_1")
@@ -50,21 +52,55 @@
     return (floats * inverse * scaling).astype(jnp.bfloat16)
 
 
-def stick_block(queries, packed, shifting, carried, allowed):
-    length, head_count, head_width = queries.shape
-    key_part = packed[:, : head_count * head_width].reshape(length, head_count, head_width)
-    value_part = packed[:, head_count * head_width :].reshape(length, head_count, head_width)
-    scores = jnp.einsum("thd,shd->hts", queries, key_part, preferred_element_type=jnp.float32)
-    scores = scores * head_width ** (-0.5) + shifting[:, None, :]
-    log_stay = jnp.where(allowed, jax.nn.log_sigmoid(-scores), 0.0)
-    between = lax.cumsum(log_stay, axis=2, reverse=True) - log_stay
-    weights = jnp.where(
-        allowed, jnp.exp(jax.nn.log_sigmoid(scores) + between + carried[:, :, None]), 0.0
-    )
-    contrib = jnp.einsum(
-        "hts,shd->thd", weights.astype(jnp.bfloat16), value_part, preferred_element_type=jnp.float32
-    )
-    return (contrib, carried + jnp.sum(log_stay, axis=2))
+def stick_step(query, keyed, valued, shifting, triangle, carried, allowed):
+    scores = lax.dot_general(
+        query, keyed, (((1,), (1,)), ((), ())), preferred_element_type=jnp.float32
+    )
+    scores = scores + shifting
+    tail = jnp.log(1.0 + jnp.exp(-jnp.abs(scores)))
+    soft = jnp.maximum(scores, 0.0) + tail
+    if allowed is not None:
+        soft = jnp.where(allowed, soft, 0.0)
+    high = soft.astype(jnp.bfloat16)
+    low = (soft - high.astype(jnp.float32)).astype(jnp.bfloat16)
+    after = jnp.dot(high, triangle, preferred_element_type=jnp.float32)
+    after = after + jnp.dot(low, triangle, preferred_element_type=jnp.float32)
+    weights = jnp.exp(jnp.minimum(scores, 0.0) - tail - (after + carried))
+    if allowed is not None:
+        weights = jnp.where(allowed, weights, 0.0)
+    contrib = jnp.dot(weights.astype(jnp.bfloat16), valued, preferred_element_type=jnp.float32)
+    return contrib, carried + after[:, :1] + soft[:, :1]
+
+
+def stick_kernel(query_ref, packed_ref, shift_ref, out_ref):
+    device = lax.axis_index(EP)
+    length, head_width = query_ref.shape
+    query = query_ref[...] * jnp.bfloat16(head_width ** (-0.5))
+    rows = lax.broadcasted_iota(jnp.int32, (length, length), 0)
+    cols = lax.broadcasted_iota(jnp.int32, (length, length), 1)
+    triangle = (rows > cols).astype(jnp.float32).astype(jnp.bfloat16)
+
+    def block(anchor, carried, allowed):
+        packed = packed_ref[anchor]
+        return stick_step(
+            query,
+            packed[:, :head_width],
+            packed[:, head_width:],
+            shift_ref[anchor],
+            triangle,
+            carried,
+            allowed,
+        )
+
+    summed, carried = block(device, jnp.zeros((length, 1), jnp.float32), cols < rows)
+
+    def visiting(offset, status):
+        running, carry_now = status
+        contrib, carry_now = block(device - offset, carry_now, None)
+        return running + contrib, carry_now
+
+    summed, carried = lax.fori_loop(1, device + 1, visiting, (summed, carried))
+    out_ref[...] = summed.astype(out_ref.dtype)
 
 
 def per_device(
@@ -90,27 +126,14 @@
     queries = jnp.dot(normed, w_query, preferred_element_type=jnp.float32).astype(jnp.bfloat16)
     key_rows = jnp.dot(normed, w_key, preferred_element_type=jnp.float32).astype(jnp.bfloat16)
     value_rows = jnp.dot(normed, w_value, preferred_element_type=jnp.float32).astype(jnp.bfloat16)
-    queries = queries.reshape(length, head_count, head_width)
     packed = jnp.concatenate([key_rows, value_rows], axis=1)
-    device = lax.axis_index(EP)
-    positions = jnp.arange(length, dtype=jnp.int32)
-    strict = (positions[None, :] < positions[:, None])[None]
-    own_shift = lax.dynamic_slice_in_dim(key_shift, device * length, length, 1)
-    summed, carried = stick_block(
-        queries, packed, own_shift, jnp.zeros((head_count, length), jnp.float32), strict
-    )
-    gathered = whole_of(packed, EP, (0, 1), 0)
-
-    def visiting(offset, status):
-        running, carry_now = status
-        anchor = device - offset
-        block_rows = lax.dynamic_slice_in_dim(gathered, anchor * length, length, 0)
-        shifting = lax.dynamic_slice_in_dim(key_shift, anchor * length, length, 1)
-        contrib, carry_now = stick_block(queries, block_rows, shifting, carry_now, True)
-        return (running + contrib, carry_now)
-
-    summed, carried = lax.fori_loop(1, device + 1, visiting, (summed, carried))
-    head_out = summed.reshape(length, head_count * head_width).astype(jnp.bfloat16)
+    gathered = all_blocks(packed, EP, (0, 1))
+    head_out = pl.pallas_call(
+        stick_kernel,
+        out_shape=jax.ShapeDtypeStruct((length, head_width), jnp.bfloat16),
+        in_specs=[pl.BlockSpec(memory_space=pltpu.VMEM)] * 3,
+        out_specs=pl.BlockSpec(memory_space=pltpu.VMEM),
+    )(queries, gathered, key_shift.reshape(-1, 1, length))
     weight_rows = w_out
     mixer_out = jnp.dot(
         gather_directly(head_out, "tp", 1), weight_rows, preferred_element_type=jnp.float32

time: 367 us -> 313 us (0.85)
  starting transfers between devices: 79 us -> 20.1 us
  waiting for transfers between devices: 185 us -> 193 us
  other arithmetic: 10.2 us -> 4.87 us
    all_to_all x1, starting transfers between devices: 73.1 us -> 14.4 us  [per_device(): lax.all_to_all(leaving, EP, split_axis=0, concat_axis=0, tiled=True)]
    all_gather x1, waiting for transfers between devices: 59.6 us -> 64.3 us  [per_device(): portion_units = lax.all_gather(hidden, 'tp', axis=2, tiled=True)]
    another operation x6 -> x2, other arithmetic: 5.85 us -> 1.2 us
  transfers between devices with their start and end apart: 6 -> 6, of which waited for: 5 -> 5; matrix products, arithmetic and copies ran while one was open for 11% -> 11% of each run, Pallas kernels for 0% -> 1%
where the time goes in v1:
time: 313 us; the launch traced here: 312 us
  waiting for transfers between devices  193 us (62%)
  blocking collectives  40.2 us (13%)
  local copies, waits for them, and re-layouts  25.5 us (8%)
  starting transfers between devices  20.1 us (6%)
  between operations  14.1 us (5%)
  matrix products  11.3 us (4%)
  other arithmetic  4.87 us (2%)
  Pallas kernels  3.51 us (1%)
    all_gather x1, waiting for transfers between devices, per_device(): expert_arrived = lax.all_gather(arrived, 'tp', axis=1, tiled=True)  72.1 us
    all_gather x1, waiting for transfers between devices, per_device(): portion_units = lax.all_gather(hidden, 'tp', axis=2, tiled=True)  64.3 us
    all_to_all x1, blocking collectives, per_device(): lax.all_to_all(own_slots, EP, split_axis=0, concat_axis=0, tiled=True)  40.2 us
    all_gather x2, waiting for transfers between devices, all_blocks(): blocks = lax.all_gather(blocks, axes[k], axis=0, tiled=True)  35.1 us
    all_to_all x1, waiting for transfers between devices, per_device(): lax.all_to_all(leaving, EP, split_axis=0, concat_axis=0, tiled=True)  21.1 us
    all_to_all x1, starting transfers between devices, per_device(): lax.all_to_all(leaving, EP, split_axis=0, concat_axis=0, tiled=True)  14.4 us
  transfers between devices with their start and end apart: 6, of which 5 were waited for; matrix products, arithmetic and copies ran while one was open for 11% of the time, Pallas kernels for 1%

profile of v1, /device:TPU:1, one launch (start us, length us, event | category | flops | bytes accessed | tf_op | source)
XLA Modules:
  0.0 312.1 jit_solution(15913427664973665195)
XLA Ops:
  7.3 1.6 fusion
  8.9 1.8 convolution_convert_fusion.2
  10.8 0.5 convolution_convert_fusion.3
  11.3 0.6 pad_maximum_fusion
  12.5 1.2 reduce-window.6
  13.9 0.2 slice_reduce_fusion
  14.6 2.4 scatter_custom_fusion
  17.1 6.0 %gather_fusion = bf16[1024,2048]{1,0:T(8,128)(2,1)} fusion(bf16[129,2048]{1,0:T(8,128)(2,1)S(1)} %concatenate.7, s32[1024]{0:T(1024)S(1)} %fusion.16), kind=kCustom, calls=%fused_computation | custom fusion | bytes 8392704 | tf_op jit(solution)/shard_map/gather | solution.py:158
  23.1 1.5 constant_dynamic-slice_fusion
  24.6 40.2 %all_to_all.15 = bf16[32,2,2048]{2,1,0:T(2,128)(2,1)S(1)} all-to-all(bf16[32,2,2048]{2,1,0:T(2,128)(2,1)S(1)} %constant_dynamic-slice_fusion), channel_id=1, replica_groups=mesh['ep_0'=16,'ep_1'=2,'tp'=16] {'ep_0','ep_1'}, dimensions={0} | all-to-all | bytes 524288 | tf_op jit(solution)/shard_map/all_to_all | solution.py:166
  64.7 0.8 copy.67
  65.6 19.6 %all-gather.12.cloned.1.call-done = bf16[4096,128]{0,1:T(8,128)(2,1)} async-done(((bf16[256,128]{0,1:T(8,128)(2,1)}), bf16[4096,128]{0,1:T(8,128)(2,1)}) %all-gather.12.cloned.1.call-update) | async-done | bytes 1048592 | tf_op jit(solution)/shard_map/all_gather | solution.py:26
  85.2 2.3 copy.70
  87.5 72.1 %all-gather.8.cloned.1.call-done = bf16[32,32,2048]{2,0,1:T(8,128)(2,1)} async-done(((bf16[32,2,2048]{2,0,1:T(8,128)(2,1)}), bf16[32,32,2048]{2,0,1:T(8,128)(2,1)}) %all-gather.8.cloned.1.call-update) | async-done | bytes 4194320 | tf_op jit(solution)/shard_map/all_gather | solution.py:167
  159.6 4.5 %copy.68 = bf16[32,32,2048]{2,1,0:T(8,128)(2,1)S(1)} copy(bf16[32,32,2048]{2,0,1:T(8,128)(2,1)} %all-gather.8.cloned.1.call-done) | data formatting | bytes 8388608 | tf_op jit(solution)/shard_map/all_gather | solution.py:167
  164.1 1.3 convolution_minimum_fusion
  165.4 2.0 fusion.5
  167.4 0.5 convolution_convert_fusion.4
  168.0 0.7 copy.61.query_ref
  168.7 15.5 %all-gather.6.cloned.1.call-done = bf16[32,256,128]{2,1,0:T(8,128)(2,1)} async-done(((bf16[16,256,128]{2,1,0:T(8,128)(2,1)}), bf16[32,256,128]{2,1,0:T(8,128)(2,1)}) %all-gather.6.cloned.1.call-update) | async-done | bytes 2097168 | tf_op jit(solution)/shard_map/all_gather | solution.py:26
  184.2 3.2 %copy.60 = bf16[16,2,256,128]{3,2,1,0:T(8,128)(2,1)} copy(bf16[16,2,256,128]{3,2,0,1:T(8,128)(2,1)} %bitcast.57) | data formatting | bytes 4194304 | tf_op jit(solution)/shard_map/transpose | solution.py:30
  187.4 3.5 %shard_map.149 = bf16[256,64]{1,0:T(8,128)(2,1)} custom-call(bf16[256,64]{1,0:T(8,128)(2,1)} %copy.61.query_ref, bf16[32,256,128]{2,1,0:T(8,128)(2,1)} %bitcast.51, f32[32,1,256]{2,1,0:T(1,128)} %bitcast.61), custom_call_target="tpu_custom_call" | custom-call | tf_op jit(solution)/shard_map/pallas_call | solution.py:131
  190.9 0.9 copy.62
  191.8 0.9 broadcast_in_dim.9
  192.7 5.5 %all-to-all-start = ((bf16[16,256,64]{1,2,0:T(8,128)(2,1)}), bf16[16,256,64]{1,2,0:T(8,128)(2,1)S(1)}, u32[]{:S(2)}, u32[]{:S(2)}) async-start(bf16[16,256,64]{1,2,0:T(8,128)(2,1)} %broadcast_in_dim.9), calls=%async_computation | async-start | bytes 1048576 | tf_op jit(solution)/shard_map/all_to_all | solution.py:39
  198.2 64.3 %all-gather.10.cloned.1.call-done = bf16[32,32,2048]{2,1,0:T(8,128)(2,1)} async-done(((bf16[32,32,128]{2,1,0:T(8,128)(2,1)}), bf16[32,32,2048]{2,1,0:T(8,128)(2,1)}) %all-gather.10.cloned.1.call-update) | async-done | bytes 4194320 | tf_op jit(solution)/shard_map/all_gather | solution.py:180
  262.5 4.2 %convolution_convert_fusion = bf16[1024,128]{1,0:T(8,128)(2,1)} fusion(bf16[1024,2048]{1,0:T(8,128)(2,1)} %bitcast.65, bf16[1,2048,128]{2,1,0:T(8,128)(2,1)S(1)} %copy-done.8), kind=kOutput, calls=%fused_computation.15 | convolution fusion | flops 537001984 | bytes 4980736 | tf_op jit(solution)/shard_map/dot_general | solution.py:183
  266.7 14.4 %all-to-all-start.2 = ((bf16[32,32,128]{2,1,0:T(8,128)(2,1)}), bf16[32,32,128]{2,1,0:T(8,128)(2,1)S(1)}, u32[]{:S(2)}, u32[]{:S(2)}) async-start(bf16[32,32,128]{2,1,0:T(8,128)(2,1)} %bitcast.17), calls=%async_computation.2 | async-start | bytes 524288 | tf_op jit(solution)/shard_map/all_to_all | solution.py:185
  281.2 1.0 convolution_convert_fusion.1
  282.2 21.1 %all-to-all-done.2 = bf16[32,32,128]{2,1,0:T(8,128)(2,1)S(1)} async-done(((bf16[32,32,128]{2,1,0:T(8,128)(2,1)}), bf16[32,32,128]{2,1,0:T(8,128)(2,1)S(1)}, u32[]{:S(2)}, u32[]{:S(2)}) %all-to-all-start.2) | async-done | bytes 262176 | tf_op jit(solution)/shard_map/all_to_all | solution.py:185
  303.3 1.3 gather_fusion.1
  304.7 0.9 fusion.12
  (53 shorter events, 1.6 us)
Async XLA Ops:
  7.2 156.9 %copy-start = (bf16[1,2048,128]{2,1,0:T(8,128)(2,1)S(1)}, bf16[1,2048,128]{2,1,0:T(8,128)(2,1)}, u32[]{:S(2)}) copy-start(bf16[1,2048,128]{2,1,0:T(8,128)(2,1)} %param.25) | copy-start | bytes 1572868
  7.2 3.6 %copy-start.2 = (bf16[256,2048]{1,0:T(8,128)(2,1)S(1)}, bf16[256,2048]{1,0:T(8,128)(2,1)}, u32[]{:S(2)}) copy-start(bf16[256,2048]{1,0:T(8,128)(2,1)} %param.14) | copy-start | bytes 3145732
  7.2 3.6 %copy-start.11 = (f32[2048]{0:T(1024)S(1)}, f32[2048]{0:T(1024)}, u32[]{:S(2)}) copy-start(f32[2048]{0:T(1024)} %param.15) | copy-start | bytes 24580
  7.2 3.6 %copy-start.9 = (bf16[2048,64]{0,1:T(8,128)(2,1)S(1)}, bf16[2048,64]{0,1:T(8,128)(2,1)}, u32[]{:S(2)}) copy-start(bf16[2048,64]{0,1:T(8,128)(2,1)} %param.17) | copy-start | bytes 786436
  7.2 78.0 %all-gather.12.cloned.1.call-start = ((), (), s32[]{:S(2)}) async-start(), calls=%async_computation.6 | async-start | bytes 1114112 | tf_op jit(solution)/shard_map/all_gather | solution.py:26
  8.9 3.1 %copy-start.5 = (s32[128,4]{0,1:T(4,128)S(1)}, s32[128,4]{0,1:T(4,128)}, u32[]{:S(2)}) copy-start(s32[128,4]{0,1:T(4,128)} %param.23) | copy-start | bytes 6148
  8.9 3.4 %copy-start.1 = (bf16[128,2048]{1,0:T(8,128)(2,1)S(1)}, bf16[128,2048]{1,0:T(8,128)(2,1)}, u32[]{:S(2)}) copy-start(bf16[128,2048]{1,0:T(8,128)(2,1)} %param.21) | copy-start | bytes 1572868
  10.8 2.9 copy-start.4
  12.0 147.6 %all-gather.8.cloned.1.call-start = ((), (), s32[]{:S(2)}) async-start(), calls=%async_computation.4 | async-start | bytes 4456448 | tf_op jit(solution)/shard_map/all_gather | solution.py:167
  65.5 118.6 %all-gather.6.cloned.1.call-start = ((), (), s32[]{:S(2)}) async-start(), calls=%async_computation.3 | async-start | bytes 3145728 | tf_op jit(solution)/shard_map/all_gather | solution.py:26
  87.5 175.0 %all-gather.10.cloned.1.call-start = ((), (), s32[]{:S(2)}) async-start(), calls=%async_computation.5 | async-start | bytes 4456448 | tf_op jit(solution)/shard_map/all_gather | solution.py:180
  164.1 1.3 copy-start.7
  165.4 2.0 copy-start.10
  187.4 75.1 %copy-start.8 = (bf16[1,2048,128]{2,1,0:T(8,128)(2,1)S(1)}, bf16[1,2048,128]{2,1,0:T(8,128)(2,1)}, u32[]{:S(2)}) copy-start(bf16[1,2048,128]{2,1,0:T(8,128)(2,1)} %param.27) | copy-start | bytes 1572868
  192.7 74.0 %all-to-all-start = ((bf16[16,256,64]{1,2,0:T(8,128)(2,1)}), bf16[16,256,64]{1,2,0:T(8,128)(2,1)S(1)}, u32[]{:S(2)}, u32[]{:S(2)}) async-start(bf16[16,256,64]{1,2,0:T(8,128)(2,1)} %broadcast_in_dim.9), calls=%async_computation | async-start | bytes 1048576 | tf_op jit(solution)/shard_map/all_to_all | solution.py:39
  262.5 18.6 %copy-start.6 = (f32[128,4]{0,1:T(4,128)S(1)}, f32[128,4]{0,1:T(4,128)}, u32[]{:S(2)}) copy-start(f32[128,4]{0,1:T(4,128)} %param.24) | copy-start | bytes 6148
  262.5 18.7 %copy-start.3 = (bf16[1024,128]{1,0:T(8,128)(2,1)S(1)}, bf16[1024,128]{1,0:T(8,128)(2,1)}, u32[]{:S(2)}) copy-start(bf16[1024,128]{1,0:T(8,128)(2,1)} %param.20) | copy-start | bytes 786436
  266.7 36.6 %all-to-all-start.2 = ((bf16[32,32,128]{2,1,0:T(8,128)(2,1)}), bf16[32,32,128]{2,1,0:T(8,128)(2,1)S(1)}, u32[]{:S(2)}, u32[]{:S(2)}) async-start(bf16[32,32,128]{2,1,0:T(8,128)(2,1)} %bitcast.17), calls=%async_computation.2 | async-start | bytes 524288 | tf_op jit(solution)/shard_map/all_to_all | solution.py:185
Sparse Core Ops, SparseCore 0:
  12.1 73.0 all-gather.11
  88.2 71.3 all-gather.7
  161.7 22.4 all-gather.5
  187.0 75.3 all-gather.9

commit v2 on v0

v2 whole, which is shorter than its diff:
```python
import jax
import jax.numpy as jnp
from jax import lax
from jax.experimental import pallas as pl
from jax.experimental.pallas import tpu as pltpu
from jax.sharding import Mesh
from jax.sharding import PartitionSpec as P

MESH = pl.DeviceIdType.MESH
EP = ("z", "c")
TP = ("y", "x")
BF = jnp.bfloat16
F32 = jnp.float32

norm_eps = 1e-06
glu_limit = 7.0
glu_alpha = 1.702

SHIFT_Z = 3


def iota(shape, dim):
    return lax.broadcasted_iota(jnp.int32, shape, dim)


def rms_scale(source, scaling):
    floats = source.astype(F32)
    inverse = lax.rsqrt(jnp.mean(floats * floats, axis=-1, keepdims=True) + norm_eps)
    return (floats * inverse * scaling).astype(BF)


def split_three(value):
    high = value.astype(BF)
    rest = value - high.astype(F32)
    middle = rest.astype(BF)
    low = (rest - middle.astype(F32)).astype(BF)
    return high, middle, low


def before_kernel(
    rows_ref,
    gain_ref,
    wq_ref,
    wk_ref,
    wv_ref,
    tokens_ref,
    token_gain_ref,
    routes_ref,
    weight_ref,
    query_ref,
    packed_ref,
    outgoing_ref,
    combine_ref,
    picked,
):
    length, width = rows_ref.shape
    head = wq_ref.shape[1]
    normed = rms_scale(rows_ref[...], gain_ref[...])
    query = jnp.dot(normed, wq_ref[...], preferred_element_type=F32).astype(BF)
    query_ref[...] = query * BF(head ** (-0.5))
    packed_ref[:, :head] = jnp.dot(normed, wk_ref[...], preferred_element_type=F32).astype(BF)
    packed_ref[:, head:] = jnp.dot(normed, wv_ref[...], preferred_element_type=F32).astype(BF)

    tokens, top = routes_ref.shape
    experts = outgoing_ref.shape[0]
    cap = combine_ref.shape[2] // experts
    part = lax.axis_index("y") * lax.axis_size("x") + lax.axis_index("x")
    normed_b = rms_scale(tokens_ref[...], token_gain_ref[...])
    chosen = routes_ref[...]
    lanes = iota((tokens, experts), 1)
    hits = jnp.zeros((tokens, experts), F32)
    for k in range(top):
        hits = hits + (chosen[:, k : k + 1] == lanes).astype(F32)
    earlier = (iota((tokens, tokens), 1) < iota((tokens, tokens), 0)).astype(F32).astype(BF)
    places = jnp.dot(earlier, hits.astype(BF), preferred_element_type=F32)
    slots = iota((tokens, experts * 2), 1)
    spots = iota((tokens, experts * cap), 1)
    select = jnp.zeros((tokens, experts * 2), F32)
    combine = jnp.zeros((tokens, experts * cap), F32)
    for k in range(top):
        expert = chosen[:, k : k + 1]
        place = jnp.sum(jnp.where(expert == lanes, places, 0.0), axis=1, keepdims=True)
        place = place.astype(jnp.int32)
        own = place - 2 * part
        wanted = jnp.where((own >= 0) & (own < 2), expert * 2 + own, -1)
        select = select + (wanted == slots).astype(F32)
        combine = combine + jnp.where(
            expert * cap + place == spots, weight_ref[:, k : k + 1], 0.0
        )
    picked[...] = lax.dot_general(
        select.astype(BF), normed_b, (((0,), (0,)), ((), ())), preferred_element_type=F32
    ).astype(BF)
    for e in range(experts):
        outgoing_ref[e] = picked[2 * e : 2 * e + 2, :]
    for n, term in enumerate(split_three(combine)):
        combine_ref[n] = term


class Plane:
    def __init__(self, piece, recv, send, here):
        self.piece, self.recv, self.send, self.here = piece, recv, send, here
        self.started = []
        self.used = [0, 0]

    def descriptor(self, part, off, axis, delta):
        x, y = self.here["x"], self.here["y"]
        slot = lax.rem(y + off["y"] + 4, 4) * 4 + lax.rem(x + off["x"] + 4, 4)
        there = dict(off)
        there[axis] -= delta
        index = (there["y"] % 4) * 4 + there["x"] % 4
        ref = self.piece(slot, part)
        number = self.used[part]
        return pltpu.make_async_remote_copy(
            src_ref=ref,
            dst_ref=ref,
            send_sem=self.send.at[part, min(number, 15)],
            recv_sem=self.recv.at[part, index],
            device_id={axis: lax.rem(self.here[axis] + delta + 4, 4)},
            device_id_type=MESH,
        )

    def put(self, part, off, axis, delta):
        copy = self.descriptor(part, off, axis, delta)
        copy.start()
        self.used[part] += 1
        self.started.append(copy)

    def take(self, part, off, axis, delta):
        x, y = self.here["x"], self.here["y"]
        slot = lax.rem(y + off["y"] + 4, 4) * 4 + lax.rem(x + off["x"] + 4, 4)
        ref = self.piece(slot, part)
        index = (off["y"] % 4) * 4 + off["x"] % 4
        pltpu.make_async_remote_copy(
            src_ref=ref,
            dst_ref=ref,
            send_sem=self.send.at[part, 15],
            recv_sem=self.recv.at[part, index],
            device_id={axis: lax.rem(self.here[axis] - delta + 4, 4)},
            device_id_type=MESH,
        ).wait_recv()

    AXES = (("x", "y"), ("y", "x"))

    @staticmethod
    def at(axes, f, s):
        return {axes[0]: f, axes[1]: s}

    def stage0(self):
        for part, axes in enumerate(self.AXES):
            for delta in (1, -1):
                self.put(part, self.at(axes, 0, 0), axes[0], delta)
        for part, axes in enumerate(self.AXES):
            for delta in (1, -1):
                self.put(part, self.at(axes, 0, 0), axes[1], delta)

    def spread(self, part, axes, f):
        for delta in (1, -1):
            self.put(part, self.at(axes, f, 0), axes[1], delta)

    def stage1(self):
        for part, axes in enumerate(self.AXES):
            self.take(part, self.at(axes, -1, 0), axes[0], 1)
            self.put(part, self.at(axes, -1, 0), axes[0], 1)
            self.spread(part, axes, -1)
        for part, axes in enumerate(self.AXES):
            self.take(part, self.at(axes, 1, 0), axes[0], -1)
            self.spread(part, axes, 1)

    def stage2(self):
        for part, axes in enumerate(self.AXES):
            self.take(part, self.at(axes, 2, 0), axes[0], 1)
            self.spread(part, axes, 2)

    def stage3(self):
        for f in (0, -1, 1, 2):
            sign = 1 if f in (0, 1) else -1
            for part, axes in enumerate(self.AXES):
                self.take(part, self.at(axes, f, -sign), axes[1], sign)
                self.put(part, self.at(axes, f, -sign), axes[1], sign)
            for part, axes in enumerate(self.AXES):
                self.take(part, self.at(axes, f, sign), axes[1], -sign)

    def stage4(self):
        for f in (0, -1, 1, 2):
            sign = 1 if f in (0, 1) else -1
            for part, axes in enumerate(self.AXES):
                self.take(part, self.at(axes, f, 2), axes[1], sign)

    def finish(self):
        for copy in self.started:
            copy.wait_send()


def main_kernel(
    query_ref,
    packed_ref,
    shift_ref,
    outgoing_ref,
    combine_ref,
    gate_ref,
    up_ref,
    down_ref,
    out_ref,
    mixer_ref,
    expert_ref,
    arrived,
    rows,
    hidden,
    leaving,
    returned,
    kv,
    heads,
    running,
    carry,
    sent_recv,
    sent_send,
    plane_recv,
    plane_send,
    kv_recv,
    kv_send,
    head_recv,
    head_send,
    back_recv,
    back_send,
):
    nz = lax.axis_size("z")
    z, c = lax.axis_index("z"), lax.axis_index("c")
    y, x = lax.axis_index("y"), lax.axis_index("x")
    here = {"x": x, "y": y}
    part = y * 4 + x
    device = z * 2 + c
    half_z = nz // 2
    started = []

    def at_z(delta):
        return lax.rem(z + delta + nz, nz)

    barrier = pltpu.get_barrier_semaphore()
    peers = 0
    for dz in range(nz):
        for k in range(2):
            if dz or k:
                pl.semaphore_signal(
                    barrier,
                    inc=1,
                    device_id={"z": at_z(dz), "c": lax.rem(c + k, 2)},
                    device_id_type=MESH,
                )
                peers += 1
    for oy in range(4):
        for ox in range(4):
            if oy or ox:
                pl.semaphore_signal(
                    barrier,
                    inc=1,
                    device_id={"y": lax.rem(y + oy, 4), "x": lax.rem(x + ox, 4)},
                    device_id_type=MESH,
                )
                peers += 1
    pl.semaphore_wait(barrier, peers)

    def dispatch(o, k):
        zt, ct = at_z(SHIFT_Z - o), lax.rem(c + k, 2)
        return pltpu.make_async_remote_copy(
            src_ref=outgoing_ref.at[zt * 2 + ct],
            dst_ref=arrived.at[o * 2 + c],
            send_sem=sent_send.at[o * 2 + k],
            recv_sem=sent_recv.at[o * 2 + k],
            device_id={"z": zt, "c": ct},
            device_id_type=MESH,
        )

    order = sorted(range(nz), key=lambda o: (o >= half_z, -abs(SHIFT_Z - o)))
    for o in order:
        for k in range(2):
            if o == SHIFT_Z and k == 0:
                continue
            copy = dispatch(o, k)
            copy.start()
            started.append(copy)
    arrived[SHIFT_Z * 2 + c] = outgoing_ref[device]

    def pass_on(block, src, index, target):
        copy = pltpu.make_async_remote_copy(
            src_ref=src,
            dst_ref=kv.at[block],
            send_sem=kv_send.at[index],
            recv_sem=kv_recv.at[index],
            device_id=target,
            device_id_type=MESH,
        )
        copy.start()
        started.append(copy)

    def got(block, index):
        pltpu.make_async_remote_copy(
            src_ref=kv.at[block],
            dst_ref=kv.at[block],
            send_sem=kv_send.at[index],
            recv_sem=kv_recv.at[index],
            device_id={"c": 1 - c},
            device_id_type=MESH,
        ).wait_recv()

    ups, downs = half_z, half_z - 1
    up0, down0, pup0, pdown0 = 0, ups, 2 * half_z, 3 * half_z + 1

    def ring(step):
        if step == 0:
            pass_on(device, packed_ref, up0, {"z": at_z(1)})
            pass_on(device, packed_ref, down0, {"z": at_z(-1)})
            pass_on(device, packed_ref, pup0, {"c": 1 - c})
            kv[device] = packed_ref[...]
            return
        block = at_z(-step) * 2 + c
        got(block, up0 + step - 1)
        if step < ups:
            pass_on(block, kv.at[block], up0 + step, {"z": at_z(1)})
        pass_on(block, kv.at[block], pup0 + step, {"c": 1 - c})
        if step <= downs:
            block = at_z(step) * 2 + c
            got(block, down0 + step - 1)
            if step < downs:
                pass_on(block, kv.at[block], down0 + step, {"z": at_z(-1)})
            pass_on(block, kv.at[block], pdown0 + step - 1, {"c": 1 - c})

    def partner_up(step):
        got(at_z(-step) * 2 + 1 - c, pup0 + step)

    def partner_down(step):
        got(at_z(step) * 2 + 1 - c, pdown0 + step - 1)

    length, head = query_ref.shape

    def stick(anchor, diagonal):
        packed = kv[anchor]
        scores = lax.dot_general(
            query_ref[...],
            packed[:, :head],
            (((1,), (1,)), ((), ())),
            preferred_element_type=F32,
        )
        scores = scores + shift_ref[anchor]
        tail = jnp.log(1.0 + jnp.exp(-jnp.abs(scores)))
        soft = jnp.maximum(scores, 0.0) + tail
        square = (length, length)
        if diagonal:
            allowed = iota(square, 1) < iota(square, 0)
            soft = jnp.where(allowed, soft, 0.0)
        triangle = (iota(square, 0) > iota(square, 1)).astype(F32).astype(BF)
        high = soft.astype(BF)
        low = (soft - high.astype(F32)).astype(BF)
        after = jnp.dot(high, triangle, preferred_element_type=F32)
        after = after + jnp.dot(low, triangle, preferred_element_type=F32)
        before = 0.0 if diagonal else carry[...]
        weights = jnp.exp(jnp.minimum(scores, 0.0) - tail - (after + before))
        if diagonal:
            weights = jnp.where(allowed, weights, 0.0)
        contrib = jnp.dot(weights.astype(BF), packed[:, head:], preferred_element_type=F32)
        total = after[:, :1] + soft[:, :1]
        if diagonal:
            running[...] = contrib
            carry[...] = total
        else:
            running[...] += contrib
            carry[...] += total

    def attend(first, last):
        low = 1 if first == 0 else 2 * first - 1 + c
        high = jnp.minimum(2 * last + c, device)

        def one(offset, none):
            stick(device - offset, False)
            return none

        lax.fori_loop(low, high + 1, one, 0)

    def gathering(number, piece):
        return Plane(piece, plane_recv.at[number], plane_send.at[number], here)

    gathers = [
        gathering(0, lambda slot, half: rows.at[0, slot * 2 + half]),
        gathering(1, lambda slot, half: rows.at[1, slot * 2 + half]),
        gathering(2, lambda slot, half: hidden.at[0, slot * 2 + half]),
        gathering(3, lambda slot, half: hidden.at[1, slot * 2 + half]),
    ]
    rows0, rows1, hidden0, hidden1 = gathers

    def lay_out(group):
        for o in range(group * half_z, (group + 1) * half_z):
            for k in range(2):
                if o == SHIFT_Z and k == 0:
                    continue
                zs, cs = at_z(o - SHIFT_Z), lax.rem(c + k, 2)
                pltpu.make_async_remote_copy(
                    src_ref=outgoing_ref.at[zs * 2 + cs],
                    dst_ref=arrived.at[o * 2 + cs],
                    send_sem=sent_send.at[o * 2 + k],
                    recv_sem=sent_recv.at[o * 2 + k],
                    device_id={"z": zs, "c": cs},
                    device_id_type=MESH,
                ).wait_recv()
        for n in range(nz):
            half, line = divmod(n, half_z)
            rows[group, part * 2 + half, 2 * line : 2 * line + 2, :] = arrived[group * nz + n]

    def expand(group):
        both = jnp.concatenate([gate_ref[...], up_ref[...]], axis=1)
        units = gate_ref.shape[1]

        def one(n, none):
            block = rows[group, pl.ds(n * 8, 8)].reshape(128, -1)
            flat = jnp.dot(block, both, preferred_element_type=F32)
            gating = jnp.minimum(flat[:, :units], glu_limit)
            linear = jnp.clip(flat[:, units:], -glu_limit, glu_limit)
            value = gating * jax.nn.sigmoid(glu_alpha * gating) * (linear + 1.0)
            where = pl.multiple_of(lax.rem(n, 2) * 128, 128)
            hidden[group, part * 2 + n // 2, pl.ds(where, 128), :] = value.astype(BF)
            return none

        lax.fori_loop(0, 4, one, 0)

    def contract(group):
        total = 512
        results = []
        for half in range(2):
            result = jnp.zeros((256, 128), F32)
            for pair in range(8):
                units = jnp.concatenate(
                    [hidden[group, 4 * pair + half], hidden[group, 4 * pair + 2 + half]], axis=1
                )
                result = result + jnp.dot(
                    units, down_ref[pair * 256 : (pair + 1) * 256], preferred_element_type=F32
                )
            results.append(result.astype(BF))
        stacked = jnp.concatenate(results, axis=0)
        to, of = iota((total, total), 0), iota((total, total), 1)
        source = ((to >> 1) & 15) * 32 + (to >> 5) * 2 + (to & 1)
        turned = jnp.dot(
            (source == of).astype(F32).astype(BF), stacked, preferred_element_type=F32
        ).astype(BF)
        leaving[group] = turned.reshape(nz, 32, 128)

    def send_back(o, k):
        zt, ct = at_z(o - SHIFT_Z), lax.rem(c + k, 2)
        group, line = divmod(o, half_z)
        return pltpu.make_async_remote_copy(
            src_ref=leaving.at[group, line * 2 + ct],
            dst_ref=returned.at[device],
            send_sem=back_send.at[o * 2 + k],
            recv_sem=back_recv.at[o * 2 + k],
            device_id={"z": zt, "c": ct},
            device_id_type=MESH,
        )

    def give_back(group):
        for o in order:
            if o // half_z != group:
                continue
            for k in range(2):
                if o == SHIFT_Z and k == 0:
                    continue
                copy = send_back(o, k)
                copy.start()
                started.append(copy)
        if group == 0:
            returned[device] = leaving[0, SHIFT_Z * 2 + c]

    def head_copy(oy, ox):
        index = ((-oy) % 4) * 4 + (-ox) % 4
        return pltpu.make_async_remote_copy(
            src_ref=heads.at[part],
            dst_ref=heads.at[part],
            send_sem=head_send.at[oy * 4 + ox],
            recv_sem=head_recv.at[index],
            device_id={"y": lax.rem(y + oy, 4), "x": lax.rem(x + ox, 4)},
            device_id_type=MESH,
        )

    def head_wait(oy, ox):
        slot = lax.rem(y + oy, 4) * 4 + lax.rem(x + ox, 4)
        pltpu.make_async_remote_copy(
            src_ref=heads.at[slot],
            dst_ref=heads.at[slot],
            send_sem=head_send.at[oy * 4 + ox],
            recv_sem=head_recv.at[oy * 4 + ox],
            device_id={"y": lax.rem(y + oy, 4), "x": lax.rem(x + ox, 4)},
            device_id_type=MESH,
        ).wait_recv()

    ring(0)
    stick(device, True)
    lay_out(0)
    rows0.stage0()
    ring(1)
    rows0.stage1()
    rows0.stage2()
    lay_out(1)
    rows1.stage0()
    ring(2)
    partner_up(0)
    partner_up(1)
    attend(0, 1)
    rows0.stage3()
    ring(3)
    rows1.stage1()
    ring(4)
    partner_up(2)
    partner_up(3)
    attend(2, 3)
    rows0.stage4()
    expand(0)
    ring(5)
    hidden0.stage0()
    rows1.stage2()
    ring(6)
    rows1.stage3()
    hidden0.stage1()
    ring(7)
    partner_up(4)
    partner_up(5)
    partner_up(6)
    attend(4, 6)
    ring(8)
    rows1.stage4()
    expand(1)
    hidden0.stage2()
    hidden1.stage0()
    hidden0.stage3()
    partner_up(7)
    partner_up(8)
    for step in range(1, downs + 1):
        partner_down(step)
    attend(7, 10)
    hidden1.stage1()
    hidden0.stage4()
    contract(0)
    hidden1.stage2()
    give_back(0)
    attend(11, nz - 1)
    hidden1.stage3()
    summed = running[...].astype(BF)
    heads[part, :, :head] = summed[: length // 2]
    heads[part, :, head:] = summed[length // 2 :]
    hidden1.stage4()
    for oy in range(4):
        for ox in range(4):
            if oy or ox:
                copy = head_copy(oy, ox)
                copy.start()
                started.append(copy)
    contract(1)
    give_back(1)
    for oy in range(4):
        for ox in range(4):
            if oy or ox:
                head_wait(oy, ox)

    mixed = jnp.zeros((length, 128), F32)
    for n in range(16):
        pair = heads[n]
        lines = jnp.concatenate([pair[:, :head], pair[:, head:]], axis=0)
        mixed = mixed + jnp.dot(
            lines, out_ref[n * head : (n + 1) * head], preferred_element_type=F32
        )
    mixer_ref[...] = mixed.astype(BF)

    for o in range(nz):
        for k in range(2):
            if o == SHIFT_Z and k == 0:
                continue
            zt, ct = at_z(SHIFT_Z - o), lax.rem(c + k, 2)
            pltpu.make_async_remote_copy(
                src_ref=returned.at[zt * 2 + ct],
                dst_ref=returned.at[zt * 2 + ct],
                send_sem=back_send.at[o * 2 + k],
                recv_sem=back_recv.at[o * 2 + k],
                device_id={"z": zt, "c": ct},
                device_id_type=MESH,
            ).wait_recv()
    table = returned[...].reshape(-1, 128)
    final = jnp.dot(combine_ref[0], table, preferred_element_type=F32)
    for n in range(1, 3):
        final = final + jnp.dot(combine_ref[n], table, preferred_element_type=F32)
    expert_ref[...] = final.astype(BF)

    for copy in started:
        copy.wait_send()
    for gather in gathers:
        gather.finish()


def per_device(
    mixer_rows,
    mixer_gain,
    w_query,
    w_key,
    w_value,
    key_shift,
    w_out,
    expert_rows,
    expert_gain,
    routes,
    route_weight,
    w_gate,
    w_up,
    w_down,
):
    length, width = mixer_rows.shape
    head = w_query.shape[1]
    tokens = expert_rows.shape[0]
    blocks = lax.axis_size("z") * 2
    cap = 2 * lax.axis_size("y") * lax.axis_size("x")
    vmem = pl.BlockSpec(memory_space=pltpu.VMEM)
    query, packed, outgoing, combine = pl.pallas_call(
        before_kernel,
        out_shape=(
            jax.ShapeDtypeStruct((length, head), BF),
            jax.ShapeDtypeStruct((length, 2 * head), BF),
            jax.ShapeDtypeStruct((blocks, 2, width), BF),
            jax.ShapeDtypeStruct((3, tokens, blocks * cap), BF),
        ),
        in_specs=[vmem] * 9,
        out_specs=(vmem,) * 4,
        scratch_shapes=[pltpu.VMEM((blocks * 2, width), BF)],
        name="before",
    )(
        mixer_rows,
        mixer_gain.reshape(1, -1),
        w_query,
        w_key,
        w_value,
        expert_rows,
        expert_gain.reshape(1, -1),
        routes,
        route_weight,
    )
    dma = pltpu.SemaphoreType.DMA
    return pl.pallas_call(
        main_kernel,
        out_shape=(
            jax.ShapeDtypeStruct((length, 128), BF),
            jax.ShapeDtypeStruct((tokens, 128), BF),
        ),
        in_specs=[vmem] * 9,
        out_specs=(vmem,) * 2,
        scratch_shapes=[
            pltpu.VMEM((blocks, 2, width), BF),
            pltpu.VMEM((2, 32, 16, width), BF),
            pltpu.VMEM((2, 32, 256, 128), BF),
            pltpu.VMEM((2, blocks // 2, 32, 128), BF),
            pltpu.VMEM((blocks, 32, 128), BF),
            pltpu.VMEM((blocks, length, 2 * head), BF),
            pltpu.VMEM((16, length // 2, 2 * head), BF),
            pltpu.VMEM((length, head), F32),
            pltpu.VMEM((length, 1), F32),
            dma((blocks,)),
            dma((blocks,)),
            dma((4, 2, 16)),
            dma((4, 2, 16)),
            dma((blocks,)),
            dma((blocks,)),
            dma((16,)),
            dma((16,)),
            dma((blocks,)),
            dma((blocks,)),
        ],
        compiler_params=pltpu.CompilerParams(
            collective_id=0, has_side_effects=True, vmem_limit_bytes=48 * 1024 * 1024
        ),
        name="main",
    )(
        query,
        packed,
        key_shift.reshape(-1, 1, length),
        outgoing,
        combine,
        w_gate[0],
        w_up[0],
        w_down[0],
        w_out,
    )


def solution(mesh):
    torus = Mesh(mesh.devices.reshape(16, 2, 4, 4), ("z", "c", "y", "x"))
    return jax.shard_map(
        per_device,
        mesh=torus,
        in_specs=(
            P(EP, None),
            P(),
            P(None, TP),
            P(None, TP),
            P(None, TP),
            P(TP, None),
            P(None, TP),
            P(EP, None),
            P(),
            P(EP, None),
            P(EP, None),
            P(EP, None, TP),
            P(EP, None, TP),
            P(EP, None, TP),
        ),
        out_specs=(P(EP, TP), P(EP, TP)),
        check_vma=False,
    )
```

time: 367 us -> 116 us (0.32)
  waiting for transfers between devices: 185 us -> 0 us
  Pallas kernels: 0 us -> 104 us
  starting transfers between devices: 79 us -> 0 us
  blocking collectives: 40.3 us -> 0 us
  local copies, waits for them, and re-layouts: 25.8 us -> 11.2 us
  between operations: 14.1 us -> 0.71 us
  matrix products: 12.4 us -> 0 us
  other arithmetic: 10.2 us -> 0 us
    all_gather x4 -> x0, waiting for transfers between devices: 163 us -> none  [the longest x1 72.1 us: per_device(): expert_arrived = lax.all_gather(arrived, 'tp', axis=1, tiled=True)]
    pallas_call x0 -> x2, Pallas kernels: none -> 104 us  [the longest x1 98.6 us: per_device(): pl.pallas_call(main_kernel, out_shape=(jax.ShapeDtypeStruct((length, 128)...]
    all_to_all x2 -> x0, starting transfers between devices: 78.6 us -> none  [the longest x1 73.1 us: per_device(): lax.all_to_all(leaving, EP, split_axis=0, concat_axis=0, tiled=True)]
    all_to_all x1 -> x0, blocking collectives: 40.3 us -> none  [per_device(): lax.all_to_all(own_slots, EP, split_axis=0, concat_axis=0, tiled=True)]
    all_to_all x2 -> x0, waiting for transfers between devices: 21.1 us -> none  [the longest x1 21.1 us: per_device(): lax.all_to_all(leaving, EP, split_axis=0, concat_axis=0, tiled=True)]
    dot_general x11 -> x0, matrix products: 12.4 us -> none  [the longest x1 4.3 us: per_device(): jnp.dot(flat_units, weight_rows, preferred_element_type=jnp.float32)]
    unnamed x25 -> x33, local copies, waits for them, and re-layouts: 2.78 us -> 11.2 us
    gather x2 -> x0, local copies, waits for them, and re-layouts: 7.35 us -> none  [the longest x1 6.02 us: per_device(): padded[owners].reshape(expert_count, capacity, rows_after_norm.shape[1])]
  transfers between devices with their start and end apart: 6 -> 0, of which waited for: 5 -> 0; matrix products, arithmetic and copies ran while one was open for 11% -> 0% of each run, Pallas kernels for 0% -> 0%
where the time goes in v2:
time: 116 us
  Pallas kernels  104 us (90%)
  local copies, waits for them, and re-layouts  11.2 us (10%)
    pallas_call x1, Pallas kernels, per_device(): pl.pallas_call(main_kernel, out_shape=(jax.ShapeDtypeStruct((length, 128)...  98.6 us
    unnamed x33, local copies, waits for them, and re-layouts  11.2 us
    pallas_call x1, Pallas kernels, per_device(): pl.pallas_call(before_kernel, out_shape=(jax.ShapeDtypeStruct((length, he...  5.16 us

profile of v2, /device:TPU:1, one launch (start us, length us, event | category | flops | bytes accessed | tf_op | source)
XLA Modules:
  0.0 115.6 jit_solution(2027059838555821299)
XLA Ops:
  0.6 0.0 copy-start.11
  0.6 0.7 copy-done.11
  1.3 0.0 copy-start.12
  1.3 0.7 copy.19.routes_ref
  2.1 0.0 copy-done.12
  2.1 0.7 copy.20.weight_ref
  2.8 0.0 copy-start.9
  2.8 2.0 %copy.16.wq_ref = bf16[2048,64]{1,0:T(8,128)(2,1)} copy(bf16[2048,64]{0,1:T(8,128)(2,1)} %param.16) | data formatting | bytes 524288 | tf_op args[2]
  4.8 0.0 copy-done.9
  4.8 0.0 copy-start.10
  4.8 1.0 copy.17.wk_ref
  5.8 0.0 copy-done.10
  5.8 1.0 copy.18.wv_ref
  6.8 0.0 copy-start.1
  6.8 0.0 copy-start.2
  6.8 0.0 copy-start.3
  6.8 0.0 copy-start.4
  6.9 0.0 copy-start.8
  6.9 5.2 %before.1 = (bf16[256,64]{1,0:T(8,128)(2,1)}, bf16[256,128]{1,0:T(8,128)(2,1)}, bf16[32,2,2048]{2,1,0:T(2,128)(2,1)}, bf16[3,128,1024]{2,1,0:T(8,128)(2,1)}) custom-call(bf16[256,2048]{1,0:T(8,128)(2,1)} %rows_ref.1, f32[1,2048]{1,0:T(1,128)} %bitcast.10, bf16[2048,64]{1,0:T(8,128)(2,1)} %copy.16.wq_ref, bf16[2048,64]{1,0:T(8,128)(2,1)} %copy.17.wk_ref, ...), custom_call_target="tpu_custom_call" | custom-call | tf_op jit(solution)/shard_map/before/pallas_call | solution.py:615
  12.0 0.0 copy-done.1
  12.0 0.0 copy-done.2
  12.0 0.0 copy-done.3
  12.0 0.0 copy-done.4
  12.1 0.0 copy-done.8
  12.1 0.0 copy-start
  12.1 1.1 copy-done
  13.2 0.9 copy-done.5
  14.1 0.8 copy-done.6
  15.0 0.8 copy-done.7
  15.8 98.6 %main.1 = (bf16[256,128]{1,0:T(8,128)(2,1)S(1)}, bf16[128,128]{1,0:T(8,128)(2,1)S(1)}) custom-call(bf16[256,64]{1,0:T(8,128)(2,1)S(1)} %copy-done.6, bf16[256,128]{1,0:T(8,128)(2,1)S(1)} %copy-done.7, f32[32,1,256]{2,1,0:T(1,128)S(1)} %bitcast.9, bf16[32,2,2048]{2,1,0:T(2,128)(2,1)S(1)} %copy-done.5, bf16[3,128,1024]{2,1,0:T(8,128)(2,1)S(1)} %copy-done, ...), custom_call_target="tpu_custom_call" | custom-call | tf_op jit(solution)/shard_map/main/pallas_call | solution.py:639
  114.4 0.6 copy.23
  115.0 0.6 copy.24
  (3 shorter events, 0.0 us)
Async XLA Ops:
  0.6 0.7 copy-start.11
  1.3 0.7 copy-start.12
  2.8 2.0 %copy-start.9 = (bf16[2048,64]{0,1:T(8,128)(2,1)S(1)}, bf16[2048,64]{0,1:T(8,128)(2,1)}, u32[]{:S(2)}) copy-start(bf16[2048,64]{0,1:T(8,128)(2,1)} %param.17) | copy-start | bytes 786436
  4.8 1.0 copy-start.10
  6.8 5.2 %copy-start.1 = (bf16[1,2048,128]{2,1,0:T(8,128)(2,1)S(1)}, bf16[1,2048,128]{2,1,0:T(8,128)(2,1)}, u32[]{:S(2)}) copy-start(bf16[1,2048,128]{2,1,0:T(8,128)(2,1)} %param.25) | copy-start | bytes 1572868
  6.8 5.2 %copy-start.2 = (bf16[1,2048,128]{2,1,0:T(8,128)(2,1)S(1)}, bf16[1,2048,128]{2,1,0:T(8,128)(2,1)}, u32[]{:S(2)}) copy-start(bf16[1,2048,128]{2,1,0:T(8,128)(2,1)} %param.26) | copy-start | bytes 1572868
  6.8 5.2 %copy-start.3 = (bf16[1,2048,128]{2,1,0:T(8,128)(2,1)S(1)}, bf16[1,2048,128]{2,1,0:T(8,128)(2,1)}, u32[]{:S(2)}) copy-start(bf16[1,2048,128]{2,1,0:T(8,128)(2,1)} %param.27) | copy-start | bytes 1572868
  6.8 5.2 %copy-start.4 = (bf16[1024,128]{1,0:T(8,128)(2,1)S(1)}, bf16[1024,128]{1,0:T(8,128)(2,1)}, u32[]{:S(2)}) copy-start(bf16[1024,128]{1,0:T(8,128)(2,1)} %out_ref.1) | copy-start | bytes 786436
  6.9 5.2 %copy-start.8 = (f32[1,8192]{1,0:T(1,128)S(1)}, f32[1,8192]{1,0:T(1,128)}, u32[]{:S(2)}) copy-start(f32[1,8192]{1,0:T(1,128)} %param.19) | copy-start | bytes 98308
  12.1 1.1 copy-start
  13.2 0.9 copy-start.5
  14.1 0.8 copy-start.6
  15.0 0.8 copy-start.7

commit v3 on v2

--- a/solution.py
+++ b/solution.py
@@ -37,63 +37,46 @@
     return high, middle, low
 
 
-def before_kernel(
-    rows_ref,
-    gain_ref,
-    wq_ref,
-    wk_ref,
-    wv_ref,
-    tokens_ref,
-    token_gain_ref,
-    routes_ref,
-    weight_ref,
-    query_ref,
-    packed_ref,
-    outgoing_ref,
-    combine_ref,
-    picked,
-):
-    length, width = rows_ref.shape
-    head = wq_ref.shape[1]
-    normed = rms_scale(rows_ref[...], gain_ref[...])
-    query = jnp.dot(normed, wq_ref[...], preferred_element_type=F32).astype(BF)
-    query_ref[...] = query * BF(head ** (-0.5))
-    packed_ref[:, :head] = jnp.dot(normed, wk_ref[...], preferred_element_type=F32).astype(BF)
-    packed_ref[:, head:] = jnp.dot(normed, wv_ref[...], preferred_element_type=F32).astype(BF)
-
-    tokens, top = routes_ref.shape
-    experts = outgoing_ref.shape[0]
-    cap = combine_ref.shape[2] // experts
-    part = lax.axis_index("y") * lax.axis_size("x") + lax.axis_index("x")
-    normed_b = rms_scale(tokens_ref[...], token_gain_ref[...])
-    chosen = routes_ref[...]
-    lanes = iota((tokens, experts), 1)
+def columns_of(routes, weights):
+    top, tokens = routes.shape
+    fill = jnp.zeros((128 - 2 * top, tokens), F32)
+    stacked = jnp.concatenate([routes.astype(F32), weights, fill], axis=0)
+    return jnp.transpose(stacked)
+
+
+def places_of(table, top, experts):
+    tokens = table.shape[0]
+    lanes = iota((tokens, experts), 1).astype(F32)
     hits = jnp.zeros((tokens, experts), F32)
     for k in range(top):
-        hits = hits + (chosen[:, k : k + 1] == lanes).astype(F32)
+        hits = hits + (table[:, k : k + 1] == lanes).astype(F32)
     earlier = (iota((tokens, tokens), 1) < iota((tokens, tokens), 0)).astype(F32).astype(BF)
-    places = jnp.dot(earlier, hits.astype(BF), preferred_element_type=F32)
-    slots = iota((tokens, experts * 2), 1)
-    spots = iota((tokens, experts * cap), 1)
+    counts = jnp.dot(earlier, hits.astype(BF), preferred_element_type=F32)
+    return [
+        jnp.sum(jnp.where(table[:, k : k + 1] == lanes, counts, 0.0), axis=1, keepdims=True)
+        for k in range(top)
+    ]
+
+
+def selection_of(table, places, top, experts, first):
+    tokens = table.shape[0]
+    slots = iota((tokens, experts * 2), 1).astype(F32)
     select = jnp.zeros((tokens, experts * 2), F32)
+    for k in range(top):
+        own = places[k] - first
+        wanted = jnp.where((own >= 0.0) & (own < 2.0), table[:, k : k + 1] * 2.0 + own, -1.0)
+        select = select + (wanted == slots).astype(F32)
+    return select.astype(BF)
+
+
+def combine_of(table, places, top, experts, cap):
+    tokens = table.shape[0]
+    spots = iota((tokens, experts * cap), 1).astype(F32)
     combine = jnp.zeros((tokens, experts * cap), F32)
     for k in range(top):
-        expert = chosen[:, k : k + 1]
-        place = jnp.sum(jnp.where(expert == lanes, places, 0.0), axis=1, keepdims=True)
-        place = place.astype(jnp.int32)
-        own = place - 2 * part
-        wanted = jnp.where((own >= 0) & (own < 2), expert * 2 + own, -1)
-        select = select + (wanted == slots).astype(F32)
-        combine = combine + jnp.where(
-            expert * cap + place == spots, weight_ref[:, k : k + 1], 0.0
-        )
-    picked[...] = lax.dot_general(
-        select.astype(BF), normed_b, (((0,), (0,)), ((), ())), preferred_element_type=F32
-    ).astype(BF)
-    for e in range(experts):
-        outgoing_ref[e] = picked[2 * e : 2 * e + 2, :]
-    for n, term in enumerate(split_three(combine)):
-        combine_ref[n] = term
+        spot = table[:, k : k + 1] * float(cap) + places[k]
+        combine = combine + jnp.where(spot == spots, table[:, top + k : top + k + 1], 0.0)
+    return split_three(combine)
 
 
 class Plane:
@@ -192,17 +175,37 @@
 
 
 def main_kernel(
-    query_ref,
-    packed_ref,
+    rows_hbm,
+    gain_ref,
+    wq_hbm,
+    wk_hbm,
+    wv_hbm,
     shift_ref,
-    outgoing_ref,
-    combine_ref,
+    out_hbm,
+    tokens_hbm,
+    token_gain_ref,
+    routes_ref,
+    weight_ref,
+    gate_hbm,
+    up_hbm,
+    down_hbm,
+    mixer_ref,
+    expert_ref,
+    source_ref,
+    wq_ref,
+    wk_ref,
+    wv_ref,
+    out_ref,
+    tokens_ref,
     gate_ref,
     up_ref,
     down_ref,
-    out_ref,
-    mixer_ref,
-    expert_ref,
+    query_ref,
+    packed_ref,
+    picked,
+    outgoing_ref,
+    combine_ref,
+    triangle_ref,
     arrived,
     rows,
     hidden,
@@ -212,6 +215,7 @@
     heads,
     running,
     carry,
+    load_sem,
     sent_recv,
     sent_send,
     plane_recv,
@@ -223,6 +227,23 @@
     back_recv,
     back_send,
 ):
+    loads = {}
+    for n, (name, src, dst) in enumerate(
+        (
+            ("tokens", tokens_hbm, tokens_ref),
+            ("rows", rows_hbm, source_ref),
+            ("q", wq_hbm, wq_ref),
+            ("k", wk_hbm, wk_ref),
+            ("v", wv_hbm, wv_ref),
+            ("gate", gate_hbm, gate_ref),
+            ("up", up_hbm, up_ref),
+            ("down", down_hbm, down_ref),
+            ("out", out_hbm, out_ref),
+        )
+    ):
+        loads[name] = pltpu.make_async_copy(src, dst, load_sem.at[n])
+        loads[name].start()
+
     nz = lax.axis_size("z")
     z, c = lax.axis_index("z"), lax.axis_index("c")
     y, x = lax.axis_index("y"), lax.axis_index("x")
@@ -257,6 +278,21 @@
                     device_id_type=MESH,
                 )
                 peers += 1
+
+    top, tokens = routes_ref.shape
+    experts = outgoing_ref.shape[0]
+    table = columns_of(routes_ref[...], weight_ref[...])
+    places = places_of(table, top, experts)
+    first = (2 * part).astype(F32)
+    select = selection_of(table, places, top, experts, first)
+    loads["tokens"].wait()
+    normed_b = rms_scale(tokens_ref[...], token_gain_ref[...])
+    picked[...] = lax.dot_general(
+        select, normed_b, (((0,), (0,)), ((), ())), preferred_element_type=F32
+    ).astype(BF)
+    for e in range(experts):
+        outgoing_ref[e] = picked[2 * e : 2 * e + 2, :]
+
     pl.semaphore_wait(barrier, peers)
 
     def dispatch(o, k):
@@ -303,36 +339,44 @@
         ).wait_recv()
 
     ups, downs = half_z, half_z - 1
-    up0, down0, pup0, pdown0 = 0, ups, 2 * half_z, 3 * half_z + 1
+    up0, down0 = -1, ups - 1
+    pup0, pdown0 = ups + downs, 2 * ups + downs
+
+    def onward(distance, src, block, sign):
+        base, most = (up0, ups) if sign > 0 else (down0, downs)
+        for hop in (2, 1):
+            if distance + hop <= most:
+                pass_on(block, src, base + distance + hop, {"z": at_z(sign * hop)})
+
+    def to_partner(distance, src, block, sign):
+        base = pup0 if sign > 0 else pdown0
+        pass_on(block, src, base + distance, {"c": 1 - c})
+
+    def arrival(distance, sign):
+        block = at_z(-sign * distance) * 2 + c
+        got(block, (up0 if sign > 0 else down0) + distance)
+        if distance % 2 == 0:
+            onward(distance, kv.at[block], block, sign)
+        to_partner(distance, kv.at[block], block, sign)
 
     def ring(step):
         if step == 0:
-            pass_on(device, packed_ref, up0, {"z": at_z(1)})
-            pass_on(device, packed_ref, down0, {"z": at_z(-1)})
-            pass_on(device, packed_ref, pup0, {"c": 1 - c})
+            onward(0, packed_ref, device, 1)
+            onward(0, packed_ref, device, -1)
+            to_partner(0, packed_ref, device, 1)
             kv[device] = packed_ref[...]
             return
-        block = at_z(-step) * 2 + c
-        got(block, up0 + step - 1)
-        if step < ups:
-            pass_on(block, kv.at[block], up0 + step, {"z": at_z(1)})
-        pass_on(block, kv.at[block], pup0 + step, {"c": 1 - c})
-        if step <= downs:
-            block = at_z(step) * 2 + c
-            got(block, down0 + step - 1)
-            if step < downs:
-                pass_on(block, kv.at[block], down0 + step, {"z": at_z(-1)})
-            pass_on(block, kv.at[block], pdown0 + step - 1, {"c": 1 - c})
-
-    def partner_up(step):
-        got(at_z(-step) * 2 + 1 - c, pup0 + step)
-
-    def partner_down(step):
-        got(at_z(step) * 2 + 1 - c, pdown0 + step - 1)
+        for distance in (2 * step, 2 * step - 1):
+            arrival(distance, 1)
+            if distance <= downs:
+                arrival(distance, -1)
+
+    def partner(distance, sign=1):
+        got(at_z(-sign * distance) * 2 + 1 - c, (pup0 if sign > 0 else pdown0) + distance)
 
     length, head = query_ref.shape
 
-    def stick(anchor, diagonal):
+    def stick(anchor, allowed=None):
         packed = kv[anchor]
         scores = lax.dot_general(
             query_ref[...],
@@ -343,37 +387,49 @@
         scores = scores + shift_ref[anchor]
         tail = jnp.log(1.0 + jnp.exp(-jnp.abs(scores)))
         soft = jnp.maximum(scores, 0.0) + tail
-        square = (length, length)
-        if diagonal:
-            allowed = iota(square, 1) < iota(square, 0)
+        if allowed is not None:
             soft = jnp.where(allowed, soft, 0.0)
-        triangle = (iota(square, 0) > iota(square, 1)).astype(F32).astype(BF)
         high = soft.astype(BF)
         low = (soft - high.astype(F32)).astype(BF)
-        after = jnp.dot(high, triangle, preferred_element_type=F32)
-        after = after + jnp.dot(low, triangle, preferred_element_type=F32)
-        before = 0.0 if diagonal else carry[...]
-        weights = jnp.exp(jnp.minimum(scores, 0.0) - tail - (after + before))
-        if diagonal:
+        after = jnp.dot(high, triangle_ref[...], preferred_element_type=F32)
+        after = after + jnp.dot(low, triangle_ref[...], preferred_element_type=F32)
+        return jnp.minimum(scores, 0.0) - tail - after, after[:, :1] + soft[:, :1], packed[:, head:]
+
+    def values_of(exponent, valued, allowed=None):
+        weights = jnp.exp(exponent)
+        if allowed is not None:
             weights = jnp.where(allowed, weights, 0.0)
-        contrib = jnp.dot(weights.astype(BF), packed[:, head:], preferred_element_type=F32)
-        total = after[:, :1] + soft[:, :1]
-        if diagonal:
-            running[...] = contrib
-            carry[...] = total
-        else:
-            running[...] += contrib
+        return jnp.dot(weights.astype(BF), valued, preferred_element_type=F32)
+
+    def attend_diagonal():
+        square = (length, length)
+        triangle_ref[...] = (iota(square, 0) > iota(square, 1)).astype(F32).astype(BF)
+        allowed = iota(square, 1) < iota(square, 0)
+        exponent, total, valued = stick(device, allowed)
+        running[...] = values_of(exponent, valued, allowed)
+        carry[...] = total
+
+    def attend_own():
+        @pl.when(c == 1)
+        def _():
+            exponent, total, valued = stick(device - 1)
+            running[...] += values_of(exponent - carry[...], valued)
             carry[...] += total
 
     def attend(first, last):
-        low = 1 if first == 0 else 2 * first - 1 + c
-        high = jnp.minimum(2 * last + c, device)
-
-        def one(offset, none):
-            stick(device - offset, False)
+        def one(distance, none):
+            near = (z - distance) * 2 + 1
+            exponent, total, valued = stick(near)
+            exponent2, total2, valued2 = stick(near - 1)
+            before = carry[...]
+            between = before + total
+            running[...] += values_of(exponent - before, valued) + values_of(
+                exponent2 - between, valued2
+            )
+            carry[...] = between + total2
             return none
 
-        lax.fori_loop(low, high + 1, one, 0)
+        lax.fori_loop(first, jnp.minimum(last, z) + 1, one, 0)
 
     def gathering(number, piece):
         return Plane(piece, plane_recv.at[number], plane_send.at[number], here)
@@ -488,74 +544,102 @@
             device_id_type=MESH,
         ).wait_recv()
 
+    def project():
+        for name in ("rows", "q", "k", "v"):
+            loads[name].wait()
+        normed = rms_scale(source_ref[...], gain_ref[...])
+
+        def product(weight_ref):
+            return lax.dot_general(
+                normed, weight_ref[...], (((1,), (1,)), ((), ())), preferred_element_type=F32
+            ).astype(BF)
+
+        query_ref[...] = product(wq_ref) * BF(head ** (-0.5))
+        packed_ref[:, :head] = product(wk_ref)
+        packed_ref[:, head:] = product(wv_ref)
+
+    def tables():
+        for n, term in enumerate(combine_of(table, places, top, experts, 32)):
+            combine_ref[n] = term
+
+    def send_heads():
+        for oy in range(4):
+            for ox in range(4):
+                if oy or ox:
+                    copy = head_copy(oy, ox)
+                    copy.start()
+                    started.append(copy)
+
+    def wait_heads():
+        for oy in range(4):
+            for ox in range(4):
+                if oy or ox:
+                    head_wait(oy, ox)
+
+    def store_heads():
+        summed = running[...].astype(BF)
+        heads[part, :, :head] = summed[: length // 2]
+        heads[part, :, head:] = summed[length // 2 :]
+
+    project()
     ring(0)
-    stick(device, True)
+    attend_diagonal()
     lay_out(0)
     rows0.stage0()
-    ring(1)
+    tables()
     rows0.stage1()
     rows0.stage2()
     lay_out(1)
     rows1.stage0()
-    ring(2)
-    partner_up(0)
-    partner_up(1)
-    attend(0, 1)
     rows0.stage3()
-    ring(3)
+    ring(1)
+    partner(0)
+    attend_own()
     rows1.stage1()
-    ring(4)
-    partner_up(2)
-    partner_up(3)
-    attend(2, 3)
+    for name in ("gate", "up", "down", "out"):
+        loads[name].wait()
     rows0.stage4()
     expand(0)
-    ring(5)
+    ring(2)
     hidden0.stage0()
     rows1.stage2()
-    ring(6)
+    partner(1)
+    partner(2)
+    attend(1, 2)
     rows1.stage3()
+    ring(3)
     hidden0.stage1()
-    ring(7)
-    partner_up(4)
-    partner_up(5)
-    partner_up(6)
-    attend(4, 6)
-    ring(8)
     rows1.stage4()
     expand(1)
+    partner(3)
+    partner(4)
+    hidden1.stage0()
+    attend(3, 4)
     hidden0.stage2()
-    hidden1.stage0()
+    ring(4)
     hidden0.stage3()
-    partner_up(7)
-    partner_up(8)
-    for step in range(1, downs + 1):
-        partner_down(step)
-    attend(7, 10)
+    partner(5)
+    partner(6)
+    attend(5, 6)
     hidden1.stage1()
+    partner(7)
+    partner(8)
+    attend(7, 8)
     hidden0.stage4()
     contract(0)
+    for step in range(1, downs + 1):
+        partner(step, -1)
+    give_back(0)
     hidden1.stage2()
-    give_back(0)
-    attend(11, nz - 1)
+    attend(9, 11)
     hidden1.stage3()
-    summed = running[...].astype(BF)
-    heads[part, :, :head] = summed[: length // 2]
-    heads[part, :, head:] = summed[length // 2 :]
+    attend(12, nz - 1)
+    store_heads()
     hidden1.stage4()
-    for oy in range(4):
-        for ox in range(4):
-            if oy or ox:
-                copy = head_copy(oy, ox)
-                copy.start()
-                started.append(copy)
+    send_heads()
     contract(1)
     give_back(1)
-    for oy in range(4):
-        for ox in range(4):
-            if oy or ox:
-                head_wait(oy, ox)
-
+    wait_heads()
     mixed = jnp.zeros((length, 128), F32)
     for n in range(16):
         pair = heads[n]
@@ -578,10 +662,10 @@
                 device_id={"z": zt, "c": ct},
                 device_id_type=MESH,
             ).wait_recv()
-    table = returned[...].reshape(-1, 128)
-    final = jnp.dot(combine_ref[0], table, preferred_element_type=F32)
+    results = returned[...].reshape(-1, 128)
+    final = jnp.dot(combine_ref[0], results, preferred_element_type=F32)
     for n in range(1, 3):
-        final = final + jnp.dot(combine_ref[n], table, preferred_element_type=F32)
+        final = final + jnp.dot(combine_ref[n], results, preferred_element_type=F32)
     expert_ref[...] = final.astype(BF)
 
     for copy in started:
@@ -612,48 +696,43 @@
     blocks = lax.axis_size("z") * 2
     cap = 2 * lax.axis_size("y") * lax.axis_size("x")
     vmem = pl.BlockSpec(memory_space=pltpu.VMEM)
-    query, packed, outgoing, combine = pl.pallas_call(
-        before_kernel,
-        out_shape=(
-            jax.ShapeDtypeStruct((length, head), BF),
-            jax.ShapeDtypeStruct((length, 2 * head), BF),
-            jax.ShapeDtypeStruct((blocks, 2, width), BF),
-            jax.ShapeDtypeStruct((3, tokens, blocks * cap), BF),
-        ),
-        in_specs=[vmem] * 9,
-        out_specs=(vmem,) * 4,
-        scratch_shapes=[pltpu.VMEM((blocks * 2, width), BF)],
-        name="before",
-    )(
-        mixer_rows,
-        mixer_gain.reshape(1, -1),
-        w_query,
-        w_key,
-        w_value,
-        expert_rows,
-        expert_gain.reshape(1, -1),
-        routes,
-        route_weight,
-    )
+    hbm = pl.BlockSpec(memory_space=pl.ANY)
     dma = pltpu.SemaphoreType.DMA
+    v = pltpu.VMEM
     return pl.pallas_call(
         main_kernel,
         out_shape=(
             jax.ShapeDtypeStruct((length, 128), BF),
             jax.ShapeDtypeStruct((tokens, 128), BF),
         ),
-        in_specs=[vmem] * 9,
+        in_specs=[hbm, vmem, hbm, hbm, hbm, vmem, hbm, hbm, vmem, vmem, vmem, hbm, hbm, hbm],
         out_specs=(vmem,) * 2,
         scratch_shapes=[
-            pltpu.VMEM((blocks, 2, width), BF),
-            pltpu.VMEM((2, 32, 16, width), BF),
-            pltpu.VMEM((2, 32, 256, 128), BF),
-            pltpu.VMEM((2, blocks // 2, 32, 128), BF),
-            pltpu.VMEM((blocks, 32, 128), BF),
-            pltpu.VMEM((blocks, length, 2 * head), BF),
-            pltpu.VMEM((16, length // 2, 2 * head), BF),
-            pltpu.VMEM((length, head), F32),
-            pltpu.VMEM((length, 1), F32),
+            v((length, width), BF),
+            v((head, width), BF),
+            v((head, width), BF),
+            v((head, width), BF),
+            v(w_out.shape, BF),
+            v((tokens, width), BF),
+            v(w_gate.shape[1:], BF),
+            v(w_up.shape[1:], BF),
+            v(w_down.shape[1:], BF),
+            v((length, head), BF),
+            v((length, 2 * head), BF),
+            v((blocks * 2, width), BF),
+            v((blocks, 2, width), BF),
+            v((3, tokens, blocks * cap), BF),
+            v((length, length), BF),
+            v((blocks, 2, width), BF),
+            v((2, 32, 16, width), BF),
+            v((2, 32, 256, 128), BF),
+            v((2, blocks // 2, 32, 128), BF),
+            v((blocks, 32, 128), BF),
+            v((blocks, length, 2 * head), BF),
+            v((16, length // 2, 2 * head), BF),
+            v((length, head), F32),
+            v((length, 1), F32),
+            dma((9,)),
             dma((blocks,)),
             dma((blocks,)),
             dma((4, 2, 16)),
@@ -666,19 +745,24 @@
             dma((blocks,)),
         ],
         compiler_params=pltpu.CompilerParams(
-            collective_id=0, has_side_effects=True, vmem_limit_bytes=48 * 1024 * 1024
+            collective_id=0, has_side_effects=True, vmem_limit_bytes=64000 * 1024
         ),
         name="main",
     )(
-        query,
-        packed,
+        mixer_rows,
+        mixer_gain.reshape(1, -1),
+        w_query.T,
+        w_key.T,
+        w_value.T,
         key_shift.reshape(-1, 1, length),
-        outgoing,
-        combine,
+        w_out,
+        expert_rows,
+        expert_gain.reshape(1, -1),
+        routes.T,
+        route_weight.T,
         w_gate[0],
         w_up[0],
         w_down[0],
-        w_out,
     )
 
 

time: 116 us -> 99.5 us (0.86)
  local copies, waits for them, and re-layouts: 11.2 us -> 2.1 us
  Pallas kernels: 104 us -> 96.6 us
    unnamed x33 -> x4, local copies, waits for them, and re-layouts: 11.2 us -> 2.1 us
    pallas_call x1 -> x0, Pallas kernels: 5.16 us -> none  [per_device(): pl.pallas_call(before_kernel, out_shape=(jax.ShapeDtypeStruct((length, he...]
    pallas_call x1, Pallas kernels: 98.6 us -> 96.6 us  [per_device(): pl.pallas_call(main_kernel, out_shape=(jax.ShapeDtypeStruct((length, 128)...]
where the time goes in v3:
time: 99.5 us; the launch traced here: 99.3 us
  Pallas kernels  96.6 us (97%)
  local copies, waits for them, and re-layouts  2.1 us (2%)
    pallas_call x1, Pallas kernels, per_device(): pl.pallas_call(main_kernel, out_shape=(jax.ShapeDtypeStruct((length, 128)...  96.6 us
    unnamed x4, local copies, waits for them, and re-layouts  2.1 us

profile of v3, /device:TPU:1, one launch (start us, length us, event | category | flops | bytes accessed | tf_op | source)
XLA Modules:
  0.0 99.3 jit_solution(1378531115046915356)
XLA Ops:
  0.6 96.6 %main.1 = (bf16[256,128]{1,0:T(8,128)(2,1)}, bf16[128,128]{1,0:T(8,128)(2,1)}) custom-call(bf16[256,2048]{1,0:T(8,128)(2,1)} %rows_hbm.1, f32[1,2048]{1,0:T(1,128)} %bitcast.18, bf16[64,2048]{1,0:T(8,128)(2,1)} %bitcast.14, bf16[64,2048]{1,0:T(8,128)(2,1)} %bitcast.15, bf16[64,2048]{1,0:T(8,128)(2,1)} %bitcast.16, f32[32,1,256]{2,1,0:T(1,128)} %bitcast.17, ...), custom_call_target="tpu_custom_call" | custom-call | tf_op jit(solution)/shard_map/main/pallas_call | solution.py:702
  97.2 0.0 copy-start
  97.2 1.5 %copy.18 = bf16[256,128]{1,0:T(8,128)(2,1)} copy(bf16[256,128]{1,0:T(8,128)(2,1)} %get-tuple-element.4) | data formatting | bytes 131072
  98.7 0.0 copy-done
  98.7 0.6 copy.19
Async XLA Ops:
  97.2 1.5 %copy-start = (bf16[128,128]{1,0:T(8,128)(2,1)S(1)}, bf16[128,128]{1,0:T(8,128)(2,1)}, u32[]{:S(2)}) copy-start(bf16[128,128]{1,0:T(8,128)(2,1)} %get-tuple-element.5) | copy-start | bytes 98308

commit v4 on v3

--- a/solution.py
+++ b/solution.py
@@ -58,14 +58,18 @@
     ]
 
 
-def selection_of(table, places, top, experts, first):
+def selection_of(table, places, top, experts, parity, firsts):
     tokens = table.shape[0]
     slots = iota((tokens, experts * 2), 1).astype(F32)
     select = jnp.zeros((tokens, experts * 2), F32)
     for k in range(top):
-        own = places[k] - first
-        wanted = jnp.where((own >= 0.0) & (own < 2.0), table[:, k : k + 1] * 2.0 + own, -1.0)
-        select = select + (wanted == slots).astype(F32)
+        expert = table[:, k : k + 1]
+        here = expert - 2.0 * jnp.floor(expert * 0.5) == parity
+        for core, first in enumerate(firsts):
+            own = places[k] - first
+            line = (expert - parity + core) * 2.0 + own
+            wanted = jnp.where(here & (own >= 0.0) & (own < 2.0), line, -1.0)
+            select = select + (wanted == slots).astype(F32)
     return select.astype(BF)
 
 
@@ -80,98 +84,117 @@
 
 
 class Plane:
-    def __init__(self, piece, recv, send, here):
-        self.piece, self.recv, self.send, self.here = piece, recv, send, here
-        self.started = []
-        self.used = [0, 0]
-
-    def descriptor(self, part, off, axis, delta):
-        x, y = self.here["x"], self.here["y"]
-        slot = lax.rem(y + off["y"] + 4, 4) * 4 + lax.rem(x + off["x"] + 4, 4)
-        there = dict(off)
-        there[axis] -= delta
-        index = (there["y"] % 4) * 4 + there["x"] % 4
-        ref = self.piece(slot, part)
-        number = self.used[part]
+    def __init__(self, pieces, order, recv, send, here, up):
+        self.pieces, self.order = pieces, order
+        self.recv, self.send, self.here, self.up = recv, send, here, up
+        self.sent = 0
+
+    def piece(self, slot, part):
+        return self.pieces.at[self.order(slot, part)]
+
+    def bulk(self, number, recv=None):
+        ref = self.pieces.at[pl.ds(0, number)]
         return pltpu.make_async_remote_copy(
             src_ref=ref,
             dst_ref=ref,
-            send_sem=self.send.at[part, min(number, 15)],
+            send_sem=self.send,
+            recv_sem=self.recv.at[0, 0] if recv is None else recv,
+            device_id={"c": 1 - self.here["c"]},
+            device_id_type=MESH,
+        )
+
+    def slot(self, f, s):
+        column = self.here["l"]
+        if f:
+            column = column + 1 - 2 * lax.rem(column, 2)
+        return lax.rem(self.here["y"] + s + 4, 4) * 4 + column
+
+    def put(self, part, f, s, where):
+        axis, delta = where
+        h = self.here
+        if axis == "x":
+            target, index = {"x": h["x"] + 1 - 2 * lax.rem(h["x"], 2)}, (1 - f) * 4 + s % 4
+        elif axis == "y":
+            target, index = {"y": lax.rem(h["y"] + delta + 4, 4)}, f * 4 + (s - delta) % 4
+        else:
+            target, index = {"c": 1 - h["c"]}, 8
+        ref = self.piece(self.slot(f, s), part)
+        copy = pltpu.make_async_remote_copy(
+            src_ref=ref,
+            dst_ref=ref,
+            send_sem=self.send,
             recv_sem=self.recv.at[part, index],
-            device_id={axis: lax.rem(self.here[axis] + delta + 4, 4)},
+            device_id=target,
             device_id_type=MESH,
         )
-
-    def put(self, part, off, axis, delta):
-        copy = self.descriptor(part, off, axis, delta)
         copy.start()
-        self.used[part] += 1
-        self.started.append(copy)
-
-    def take(self, part, off, axis, delta):
-        x, y = self.here["x"], self.here["y"]
-        slot = lax.rem(y + off["y"] + 4, 4) * 4 + lax.rem(x + off["x"] + 4, 4)
-        ref = self.piece(slot, part)
-        index = (off["y"] % 4) * 4 + off["x"] % 4
+        self.sent += 1
+
+    def take(self, part, f, s):
+        ref = self.piece(self.slot(f, s), part)
         pltpu.make_async_remote_copy(
             src_ref=ref,
             dst_ref=ref,
-            send_sem=self.send.at[part, 15],
-            recv_sem=self.recv.at[part, index],
-            device_id={axis: lax.rem(self.here[axis] - delta + 4, 4)},
+            send_sem=self.send,
+            recv_sem=self.recv.at[part, f * 4 + s % 4],
+            device_id={"c": 1 - self.here["c"]},
             device_id_type=MESH,
         ).wait_recv()
 
-    AXES = (("x", "y"), ("y", "x"))
-
-    @staticmethod
-    def at(axes, f, s):
-        return {axes[0]: f, axes[1]: s}
-
-    def stage0(self):
-        for part, axes in enumerate(self.AXES):
-            for delta in (1, -1):
-                self.put(part, self.at(axes, 0, 0), axes[0], delta)
-        for part, axes in enumerate(self.AXES):
-            for delta in (1, -1):
-                self.put(part, self.at(axes, 0, 0), axes[1], delta)
-
-    def spread(self, part, axes, f):
+    def along_y(self, part, f):
         for delta in (1, -1):
-            self.put(part, self.at(axes, f, 0), axes[1], delta)
+            self.put(part, f, 0, ("y", delta))
+
+    def stage0a(self):
+        self.put(0, 0, 0, ("x", 0))
+        self.along_y(1, 0)
+
+    def stage0b(self):
+        self.along_y(0, 0)
+        self.put(1, 0, 0, ("x", 0))
+        for part in range(2):
+            self.put(part, 0, 0, ("c", 0))
 
     def stage1(self):
-        for part, axes in enumerate(self.AXES):
-            self.take(part, self.at(axes, -1, 0), axes[0], 1)
-            self.put(part, self.at(axes, -1, 0), axes[0], 1)
-            self.spread(part, axes, -1)
-        for part, axes in enumerate(self.AXES):
-            self.take(part, self.at(axes, 1, 0), axes[0], -1)
-            self.spread(part, axes, 1)
+        up = self.up
+        self.take(1, 0, -up)
+        self.put(1, 0, -up, ("y", up))
+        self.put(1, 0, -up, ("x", 0))
+        self.take(0, 1, 0)
+        self.along_y(0, 1)
+        self.take(1, 0, up)
+        self.put(1, 0, up, ("x", 0))
+        self.put(0, 1, 0, ("c", 0))
+        self.put(1, 0, -up, ("c", 0))
+        self.put(1, 0, up, ("c", 0))
 
     def stage2(self):
-        for part, axes in enumerate(self.AXES):
-            self.take(part, self.at(axes, 2, 0), axes[0], 1)
-            self.spread(part, axes, 2)
+        for f, sign in ((0, -self.up), (1, self.up)):
+            self.take(0, f, -sign)
+            self.put(0, f, -sign, ("y", sign))
+            self.put(0, f, -sign, ("c", 0))
+            if f == 0:
+                self.take(1, 0, 2)
+                self.put(1, 0, 2, ("x", 0))
+                self.put(1, 0, 2, ("c", 0))
 
     def stage3(self):
-        for f in (0, -1, 1, 2):
-            sign = 1 if f in (0, 1) else -1
-            for part, axes in enumerate(self.AXES):
-                self.take(part, self.at(axes, f, -sign), axes[1], sign)
-                self.put(part, self.at(axes, f, -sign), axes[1], sign)
-            for part, axes in enumerate(self.AXES):
-                self.take(part, self.at(axes, f, sign), axes[1], -sign)
+        for f, sign in ((0, -self.up), (1, self.up)):
+            self.take(0, f, sign)
+            self.put(0, f, sign, ("c", 0))
+        for s in (0, -self.up, self.up, 2):
+            self.take(1, 1, s)
+            self.put(1, 1, s, ("c", 0))
 
     def stage4(self):
-        for f in (0, -1, 1, 2):
-            sign = 1 if f in (0, 1) else -1
-            for part, axes in enumerate(self.AXES):
-                self.take(part, self.at(axes, f, 2), axes[1], sign)
+        for f in range(2):
+            self.take(0, f, 2)
+            self.put(0, f, 2, ("c", 0))
+        for part in range(2):
+            self.bulk(8, self.recv.at[part, 8]).wait_recv()
 
     def finish(self):
-        for copy in self.started:
-            copy.wait_send()
+        self.bulk(self.sent).wait_send()
 
 
 def main_kernel(
@@ -216,6 +239,8 @@
     running,
     carry,
     load_sem,
+    trade_recv,
+    trade_send,
     sent_recv,
     sent_send,
     plane_recv,
@@ -235,9 +260,9 @@
             ("q", wq_hbm, wq_ref),
             ("k", wk_hbm, wk_ref),
             ("v", wv_hbm, wv_ref),
-            ("gate", gate_hbm, gate_ref),
-            ("up", up_hbm, up_ref),
-            ("down", down_hbm, down_ref),
+            ("gate", gate_hbm, gate_ref.at[0]),
+            ("up", up_hbm, up_ref.at[0]),
+            ("down", down_hbm, down_ref.at[0]),
             ("out", out_hbm, out_ref),
         )
     ):
@@ -247,11 +272,15 @@
     nz = lax.axis_size("z")
     z, c = lax.axis_index("z"), lax.axis_index("c")
     y, x = lax.axis_index("y"), lax.axis_index("x")
-    here = {"x": x, "y": y}
+    side = x // 2
+    traded = lax.rem(side + c, 2)
+    column = x + traded * (3 - 2 * x)
+    here = {"x": x, "y": y, "c": c, "l": column}
+    spot = y * 4 + column
+    expert_here = z * 2 + side
     part = y * 4 + x
     device = z * 2 + c
     half_z = nz // 2
-    started = []
 
     def at_z(delta):
         return lax.rem(z + delta + nz, nz)
@@ -268,6 +297,15 @@
                     device_id_type=MESH,
                 )
                 peers += 1
+    for dz in range(nz):
+        for k in range(2):
+            pl.semaphore_signal(
+                barrier,
+                inc=1,
+                device_id={"z": at_z(dz), "c": lax.rem(c + k, 2), "x": 3 - x},
+                device_id_type=MESH,
+            )
+            peers += 1
     for oy in range(4):
         for ox in range(4):
             if oy or ox:
@@ -283,8 +321,10 @@
     experts = outgoing_ref.shape[0]
     table = columns_of(routes_ref[...], weight_ref[...])
     places = places_of(table, top, experts)
-    first = (2 * part).astype(F32)
-    select = selection_of(table, places, top, experts, first)
+    firsts = [
+        (2 * (y * 4 + x + lax.rem(side + core, 2) * (3 - 2 * x))).astype(F32) for core in range(2)
+    ]
+    select = selection_of(table, places, top, experts, side.astype(F32), firsts)
     loads["tokens"].wait()
     normed_b = rms_scale(tokens_ref[...], token_gain_ref[...])
     picked[...] = lax.dot_general(
@@ -300,39 +340,62 @@
         return pltpu.make_async_remote_copy(
             src_ref=outgoing_ref.at[zt * 2 + ct],
             dst_ref=arrived.at[o * 2 + c],
-            send_sem=sent_send.at[o * 2 + k],
-            recv_sem=sent_recv.at[o * 2 + k],
+            send_sem=sent_send,
+            recv_sem=sent_recv.at[o // half_z],
             device_id={"z": zt, "c": ct},
             device_id_type=MESH,
         )
 
-    order = sorted(range(nz), key=lambda o: (o >= half_z, -abs(SHIFT_Z - o)))
-    for o in order:
-        for k in range(2):
-            if o == SHIFT_Z and k == 0:
+    order = sorted(range(nz), key=lambda o: -min((o - SHIFT_Z) % nz, (SHIFT_Z - o) % nz))
+    def send_out(group):
+        for o in order:
+            if o // half_z != group:
                 continue
-            copy = dispatch(o, k)
-            copy.start()
-            started.append(copy)
-    arrived[SHIFT_Z * 2 + c] = outgoing_ref[device]
+            for k in range(2):
+                if o == SHIFT_Z and k == 0:
+                    continue
+                dispatch(o, k).start()
+        if group == 0:
+            arrived[SHIFT_Z * 2 + c] = outgoing_ref[device]
+
+    def traded_copy(n):
+        src, dst = ((gate_hbm, gate_ref), (up_hbm, up_ref), (down_hbm, down_ref))[n]
+        return pltpu.make_async_remote_copy(
+            src_ref=src,
+            dst_ref=dst.at[1],
+            send_sem=trade_send,
+            recv_sem=trade_recv.at[n],
+            device_id={"x": 3 - x, "c": 1 - c},
+            device_id_type=MESH,
+        )
+
+    def trade():
+        @pl.when(traded == 1)
+        def _():
+            for n in range(3):
+                traded_copy(n).start()
+
+    def traded_in(numbers):
+        @pl.when(traded == 1)
+        def _():
+            for n in numbers:
+                traded_copy(n).wait_recv()
 
     def pass_on(block, src, index, target):
-        copy = pltpu.make_async_remote_copy(
+        pltpu.make_async_remote_copy(
             src_ref=src,
             dst_ref=kv.at[block],
-            send_sem=kv_send.at[index],
+            send_sem=kv_send,
             recv_sem=kv_recv.at[index],
             device_id=target,
             device_id_type=MESH,
-        )
-        copy.start()
-        started.append(copy)
+        ).start()
 
     def got(block, index):
         pltpu.make_async_remote_copy(
             src_ref=kv.at[block],
             dst_ref=kv.at[block],
-            send_sem=kv_send.at[index],
+            send_sem=kv_send,
             recv_sem=kv_recv.at[index],
             device_id={"c": 1 - c},
             device_id_type=MESH,
@@ -364,7 +427,6 @@
             onward(0, packed_ref, device, 1)
             onward(0, packed_ref, device, -1)
             to_partner(0, packed_ref, device, 1)
-            kv[device] = packed_ref[...]
             return
         for distance in (2 * step, 2 * step - 1):
             arrival(distance, 1)
@@ -431,38 +493,39 @@
 
         lax.fori_loop(first, jnp.minimum(last, z) + 1, one, 0)
 
-    def gathering(number, piece):
-        return Plane(piece, plane_recv.at[number], plane_send.at[number], here)
+    def gathering(number, pieces):
+        sign = 1 if number in (0, 3) else -1
+
+        def order(slot, part):
+            return slot * 2 + part
+
+        return Plane(pieces, order, plane_recv.at[number], plane_send.at[number], here, sign)
 
     gathers = [
-        gathering(0, lambda slot, half: rows.at[0, slot * 2 + half]),
-        gathering(1, lambda slot, half: rows.at[1, slot * 2 + half]),
-        gathering(2, lambda slot, half: hidden.at[0, slot * 2 + half]),
-        gathering(3, lambda slot, half: hidden.at[1, slot * 2 + half]),
+        gathering(0, rows.at[0]),
+        gathering(1, rows.at[1]),
+        gathering(2, hidden.at[0]),
+        gathering(3, hidden.at[1]),
     ]
     rows0, rows1, hidden0, hidden1 = gathers
 
     def lay_out(group):
-        for o in range(group * half_z, (group + 1) * half_z):
-            for k in range(2):
-                if o == SHIFT_Z and k == 0:
-                    continue
-                zs, cs = at_z(o - SHIFT_Z), lax.rem(c + k, 2)
-                pltpu.make_async_remote_copy(
-                    src_ref=outgoing_ref.at[zs * 2 + cs],
-                    dst_ref=arrived.at[o * 2 + cs],
-                    send_sem=sent_send.at[o * 2 + k],
-                    recv_sem=sent_recv.at[o * 2 + k],
-                    device_id={"z": zs, "c": cs},
-                    device_id_type=MESH,
-                ).wait_recv()
+        ref = arrived.at[pl.ds(0, nz - 1 + group)]
+        pltpu.make_async_remote_copy(
+            src_ref=ref,
+            dst_ref=ref,
+            send_sem=sent_send,
+            recv_sem=sent_recv.at[group],
+            device_id={"c": 1 - c},
+            device_id_type=MESH,
+        ).wait_recv()
         for n in range(nz):
             half, line = divmod(n, half_z)
-            rows[group, part * 2 + half, 2 * line : 2 * line + 2, :] = arrived[group * nz + n]
+            rows[group, spot * 2 + half, 2 * line : 2 * line + 2, :] = arrived[group * nz + n]
 
     def expand(group):
-        both = jnp.concatenate([gate_ref[...], up_ref[...]], axis=1)
-        units = gate_ref.shape[1]
+        both = jnp.concatenate([gate_ref[traded], up_ref[traded]], axis=1)
+        units = gate_ref.shape[2]
 
         def one(n, none):
             block = rows[group, pl.ds(n * 8, 8)].reshape(128, -1)
@@ -471,7 +534,7 @@
             linear = jnp.clip(flat[:, units:], -glu_limit, glu_limit)
             value = gating * jax.nn.sigmoid(glu_alpha * gating) * (linear + 1.0)
             where = pl.multiple_of(lax.rem(n, 2) * 128, 128)
-            hidden[group, part * 2 + n // 2, pl.ds(where, 128), :] = value.astype(BF)
+            hidden[group, spot * 2 + n // 2, pl.ds(where, 128), :] = value.astype(BF)
             return none
 
         lax.fori_loop(0, 4, one, 0)
@@ -486,7 +549,7 @@
                     [hidden[group, 4 * pair + half], hidden[group, 4 * pair + 2 + half]], axis=1
                 )
                 result = result + jnp.dot(
-                    units, down_ref[pair * 256 : (pair + 1) * 256], preferred_element_type=F32
+                    units, down_ref[traded, pair * 256 : (pair + 1) * 256], preferred_element_type=F32
                 )
             results.append(result.astype(BF))
         stacked = jnp.concatenate(results, axis=0)
@@ -502,10 +565,10 @@
         group, line = divmod(o, half_z)
         return pltpu.make_async_remote_copy(
             src_ref=leaving.at[group, line * 2 + ct],
-            dst_ref=returned.at[device],
-            send_sem=back_send.at[o * 2 + k],
-            recv_sem=back_recv.at[o * 2 + k],
-            device_id={"z": zt, "c": ct},
+            dst_ref=returned.at[expert_here],
+            send_sem=back_send,
+            recv_sem=back_recv,
+            device_id={"z": zt, "c": ct, "x": column},
             device_id_type=MESH,
         )
 
@@ -515,34 +578,49 @@
                 continue
             for k in range(2):
                 if o == SHIFT_Z and k == 0:
+
+                    @pl.when(traded == 1)
+                    def _():
+                        send_back(SHIFT_Z, 0).start()
+
+                    @pl.when(traded == 0)
+                    def _():
+                        returned[expert_here] = leaving[0, SHIFT_Z * 2 + c]
+
                     continue
-                copy = send_back(o, k)
-                copy.start()
-                started.append(copy)
-        if group == 0:
-            returned[device] = leaving[0, SHIFT_Z * 2 + c]
+                send_back(o, k).start()
+
+    def bulk(ref, send, recv):
+        return pltpu.make_async_remote_copy(
+            src_ref=ref,
+            dst_ref=ref,
+            send_sem=send,
+            recv_sem=recv,
+            device_id={"c": 1 - c},
+            device_id_type=MESH,
+        )
+
+    def of_all(wait):
+        @pl.when(traded == 1)
+        def _():
+            wait(bulk(returned.at[pl.ds(0, 2 * nz)], back_send, back_recv))
+
+        @pl.when(traded == 0)
+        def _():
+            wait(bulk(returned.at[pl.ds(0, 2 * nz - 1)], back_send, back_recv))
+
+    def take_back():
+        of_all(lambda copy: copy.wait_recv())
 
     def head_copy(oy, ox):
-        index = ((-oy) % 4) * 4 + (-ox) % 4
         return pltpu.make_async_remote_copy(
             src_ref=heads.at[part],
             dst_ref=heads.at[part],
-            send_sem=head_send.at[oy * 4 + ox],
-            recv_sem=head_recv.at[index],
+            send_sem=head_send,
+            recv_sem=head_recv,
             device_id={"y": lax.rem(y + oy, 4), "x": lax.rem(x + ox, 4)},
             device_id_type=MESH,
         )
-
-    def head_wait(oy, ox):
-        slot = lax.rem(y + oy, 4) * 4 + lax.rem(x + ox, 4)
-        pltpu.make_async_remote_copy(
-            src_ref=heads.at[slot],
-            dst_ref=heads.at[slot],
-            send_sem=head_send.at[oy * 4 + ox],
-            recv_sem=head_recv.at[oy * 4 + ox],
-            device_id={"y": lax.rem(y + oy, 4), "x": lax.rem(x + ox, 4)},
-            device_id_type=MESH,
-        ).wait_recv()
 
     def project():
         for name in ("rows", "q", "k", "v"):
@@ -557,6 +635,7 @@
         query_ref[...] = product(wq_ref) * BF(head ** (-0.5))
         packed_ref[:, :head] = product(wk_ref)
         packed_ref[:, head:] = product(wv_ref)
+        kv[device] = packed_ref[...]
 
     def tables():
         for n, term in enumerate(combine_of(table, places, top, experts, 32)):
@@ -566,112 +645,118 @@
         for oy in range(4):
             for ox in range(4):
                 if oy or ox:
-                    copy = head_copy(oy, ox)
-                    copy.start()
-                    started.append(copy)
+                    head_copy(oy, ox).start()
 
     def wait_heads():
-        for oy in range(4):
-            for ox in range(4):
-                if oy or ox:
-                    head_wait(oy, ox)
+        bulk(heads.at[pl.ds(0, 15)], head_send, head_recv).wait_recv()
 
     def store_heads():
         summed = running[...].astype(BF)
         heads[part, :, :head] = summed[: length // 2]
         heads[part, :, head:] = summed[length // 2 :]
 
+    def mix():
+        mixed = jnp.zeros((length, 128), F32)
+        for n in range(16):
+            pair = heads[n]
+            lines = jnp.concatenate([pair[:, :head], pair[:, head:]], axis=0)
+            mixed = mixed + jnp.dot(
+                lines, out_ref[n * head : (n + 1) * head], preferred_element_type=F32
+            )
+        mixer_ref[...] = mixed.astype(BF)
+
+    def combine():
+        results = returned[...].reshape(-1, 128)
+        final = jnp.dot(combine_ref[0], results, preferred_element_type=F32)
+        for n in range(1, 3):
+            final = final + jnp.dot(combine_ref[n], results, preferred_element_type=F32)
+        expert_ref[...] = final.astype(BF)
+
+    def settle():
+        bulk(arrived.at[pl.ds(0, 2 * nz - 1)], sent_send, sent_recv.at[0]).wait_send()
+        bulk(kv.at[pl.ds(0, 2 * (ups + downs) + 1)], kv_send, kv_recv.at[0]).wait_send()
+        bulk(heads.at[pl.ds(0, 15)], head_send, head_recv).wait_send()
+        of_all(lambda copy: copy.wait_send())
+        for gather in gathers:
+            gather.finish()
+
+        @pl.when(traded == 1)
+        def _():
+            bulk(gate_ref, trade_send, trade_recv.at[0]).wait_send()
+            bulk(down_ref.at[0], trade_send, trade_recv.at[0]).wait_send()
+
+    send_out(0)
+    trade()
     project()
-    ring(0)
+    send_out(1)
     attend_diagonal()
     lay_out(0)
-    rows0.stage0()
+    rows0.stage0a()
+    rows0.stage0b()
+    ring(0)
     tables()
     rows0.stage1()
     rows0.stage2()
+    for name in ("gate", "up", "down", "out"):
+        loads[name].wait()
+    ring(1)
     lay_out(1)
-    rows1.stage0()
+    rows1.stage0a()
+    rows1.stage0b()
     rows0.stage3()
-    ring(1)
+    rows1.stage1()
+    rows0.stage4()
+    traded_in((0, 1))
+    expand(0)
+    hidden0.stage0a()
+    ring(2)
+    rows1.stage2()
+    hidden0.stage0b()
     partner(0)
     attend_own()
-    rows1.stage1()
-    for name in ("gate", "up", "down", "out"):
-        loads[name].wait()
-    rows0.stage4()
-    expand(0)
-    ring(2)
-    hidden0.stage0()
-    rows1.stage2()
     partner(1)
     partner(2)
     attend(1, 2)
     rows1.stage3()
-    ring(3)
     hidden0.stage1()
     rows1.stage4()
     expand(1)
+    hidden1.stage0a()
+    ring(3)
     partner(3)
     partner(4)
-    hidden1.stage0()
     attend(3, 4)
     hidden0.stage2()
+    hidden1.stage0b()
+    hidden0.stage3()
+    hidden1.stage1()
     ring(4)
-    hidden0.stage3()
     partner(5)
     partner(6)
     attend(5, 6)
-    hidden1.stage1()
+    hidden0.stage4()
+    traded_in((2,))
+    contract(0)
+    give_back(0)
     partner(7)
     partner(8)
     attend(7, 8)
-    hidden0.stage4()
-    contract(0)
+    hidden1.stage2()
     for step in range(1, downs + 1):
         partner(step, -1)
-    give_back(0)
-    hidden1.stage2()
     attend(9, 11)
     hidden1.stage3()
     attend(12, nz - 1)
     store_heads()
+    send_heads()
     hidden1.stage4()
-    send_heads()
     contract(1)
     give_back(1)
     wait_heads()
-    mixed = jnp.zeros((length, 128), F32)
-    for n in range(16):
-        pair = heads[n]
-        lines = jnp.concatenate([pair[:, :head], pair[:, head:]], axis=0)
-        mixed = mixed + jnp.dot(
-            lines, out_ref[n * head : (n + 1) * head], preferred_element_type=F32
-        )
-    mixer_ref[...] = mixed.astype(BF)
-
-    for o in range(nz):
-        for k in range(2):
-            if o == SHIFT_Z and k == 0:
-                continue
-            zt, ct = at_z(SHIFT_Z - o), lax.rem(c + k, 2)
-            pltpu.make_async_remote_copy(
-                src_ref=returned.at[zt * 2 + ct],
-                dst_ref=returned.at[zt * 2 + ct],
-                send_sem=back_send.at[o * 2 + k],
-                recv_sem=back_recv.at[o * 2 + k],
-                device_id={"z": zt, "c": ct},
-                device_id_type=MESH,
-            ).wait_recv()
-    results = returned[...].reshape(-1, 128)
-    final = jnp.dot(combine_ref[0], results, preferred_element_type=F32)
-    for n in range(1, 3):
-        final = final + jnp.dot(combine_ref[n], results, preferred_element_type=F32)
-    expert_ref[...] = final.astype(BF)
-
-    for copy in started:
-        copy.wait_send()
-    for gather in gathers:
-        gather.finish()
+    mix()
+    take_back()
+    combine()
+    settle()
 
 
 def per_device(
@@ -714,9 +799,9 @@
             v((head, width), BF),
             v(w_out.shape, BF),
             v((tokens, width), BF),
-            v(w_gate.shape[1:], BF),
-            v(w_up.shape[1:], BF),
-            v(w_down.shape[1:], BF),
+            v((2, *w_gate.shape[1:]), BF),
+            v((2, *w_up.shape[1:]), BF),
+            v((2, *w_down.shape[1:]), BF),
             v((length, head), BF),
             v((length, 2 * head), BF),
             v((blocks * 2, width), BF),
@@ -733,16 +818,18 @@
             v((length, head), F32),
             v((length, 1), F32),
             dma((9,)),
-            dma((blocks,)),
-            dma((blocks,)),
-            dma((4, 2, 16)),
-            dma((4, 2, 16)),
-            dma((blocks,)),
-            dma((blocks,)),
-            dma((16,)),
-            dma((16,)),
-            dma((blocks,)),
-            dma((blocks,)),
+            dma((3,)),
+            dma,
+            dma((2,)),
+            dma,
+            dma((4, 2, 9)),
+            dma((4,)),
+            dma((blocks - 1,)),
+            dma,
+            dma,
+            dma,
+            dma,
+            dma,
         ],
         compiler_params=pltpu.CompilerParams(
             collective_id=0, has_side_effects=True, vmem_limit_bytes=64000 * 1024

time: 99.5 us -> 84.9 us (0.85)
  Pallas kernels: 96.6 us -> 81.3 us
    pallas_call x1, Pallas kernels: 96.6 us -> 81.3 us  [per_device(): pl.pallas_call(main_kernel, out_shape=(jax.ShapeDtypeStruct((length, 128)...]
where the time goes in v4:
time: 84.9 us; the launch traced here: 84 us
  Pallas kernels  81.3 us (96%)
  local copies, waits for them, and re-layouts  2.1 us (2%)
    pallas_call x1, Pallas kernels, per_device(): pl.pallas_call(main_kernel, out_shape=(jax.ShapeDtypeStruct((length, 128)...  81.3 us
    unnamed x4, local copies, waits for them, and re-layouts  2.1 us

profile of v4, /device:TPU:1, one launch (start us, length us, event | category | flops | bytes accessed | tf_op | source)
XLA Modules:
  0.0 84.0 jit_solution(8705831864763297687)
XLA Ops:
  0.6 81.3 %main.1 = (bf16[256,128]{1,0:T(8,128)(2,1)}, bf16[128,128]{1,0:T(8,128)(2,1)}) custom-call(bf16[256,2048]{1,0:T(8,128)(2,1)} %rows_hbm.1, f32[1,2048]{1,0:T(1,128)} %bitcast.18, bf16[64,2048]{1,0:T(8,128)(2,1)} %bitcast.14, bf16[64,2048]{1,0:T(8,128)(2,1)} %bitcast.15, bf16[64,2048]{1,0:T(8,128)(2,1)} %bitcast.16, f32[32,1,256]{2,1,0:T(1,128)} %bitcast.17, ...), custom_call_target="tpu_custom_call" | custom-call | tf_op jit(solution)/shard_map/main/pallas_call | solution.py:787
  81.9 0.0 copy-start
  81.9 1.5 %copy.18 = bf16[256,128]{1,0:T(8,128)(2,1)} copy(bf16[256,128]{1,0:T(8,128)(2,1)} %get-tuple-element.4) | data formatting | bytes 131072
  83.4 0.0 copy-done
  83.4 0.6 copy.19
Async XLA Ops:
  81.9 1.5 %copy-start = (bf16[128,128]{1,0:T(8,128)(2,1)S(1)}, bf16[128,128]{1,0:T(8,128)(2,1)}, u32[]{:S(2)}) copy-start(bf16[128,128]{1,0:T(8,128)(2,1)} %get-tuple-element.5) | copy-start | bytes 98308

commit v5 on v4

--- a/solution.py
+++ b/solution.py
@@ -16,7 +16,9 @@
 glu_limit = 7.0
 glu_alpha = 1.702
 
-SHIFT_Z = 3
+OFFSETS = (-1, 0, 1, 2, 8, 7, -7, -6, 6, 5, -5, -4, 4, 3, -3, -2)
+GROUPS = 4
+OWN = OFFSETS.index(0)
 
 
 def iota(shape, dim):
@@ -190,6 +192,8 @@
         for f in range(2):
             self.take(0, f, 2)
             self.put(0, f, 2, ("c", 0))
+
+    def stage5(self):
         for part in range(2):
             self.bulk(8, self.recv.at[part, 8]).wait_recv()
 
@@ -281,6 +285,7 @@
     part = y * 4 + x
     device = z * 2 + c
     half_z = nz // 2
+    chips = nz // GROUPS
 
     def at_z(delta):
         return lax.rem(z + delta + nz, nz)
@@ -336,27 +341,27 @@
     pl.semaphore_wait(barrier, peers)
 
     def dispatch(o, k):
-        zt, ct = at_z(SHIFT_Z - o), lax.rem(c + k, 2)
+        zt, ct = at_z(-OFFSETS[o]), lax.rem(c + k, 2)
         return pltpu.make_async_remote_copy(
             src_ref=outgoing_ref.at[zt * 2 + ct],
             dst_ref=arrived.at[o * 2 + c],
             send_sem=sent_send,
-            recv_sem=sent_recv.at[o // half_z],
+            recv_sem=sent_recv.at[o // chips],
             device_id={"z": zt, "c": ct},
             device_id_type=MESH,
         )
 
-    order = sorted(range(nz), key=lambda o: -min((o - SHIFT_Z) % nz, (SHIFT_Z - o) % nz))
+    def order_of(group):
+        return sorted(range(group * chips, (group + 1) * chips), key=lambda o: -abs(OFFSETS[o]))
+
     def send_out(group):
-        for o in order:
-            if o // half_z != group:
-                continue
+        for o in order_of(group):
             for k in range(2):
-                if o == SHIFT_Z and k == 0:
+                if o == OWN and k == 0:
                     continue
                 dispatch(o, k).start()
         if group == 0:
-            arrived[SHIFT_Z * 2 + c] = outgoing_ref[device]
+            arrived[OWN * 2 + c] = outgoing_ref[device]
 
     def traded_copy(n):
         src, dst = ((gate_hbm, gate_ref), (up_hbm, up_ref), (down_hbm, down_ref))[n]
@@ -451,10 +456,7 @@
         soft = jnp.maximum(scores, 0.0) + tail
         if allowed is not None:
             soft = jnp.where(allowed, soft, 0.0)
-        high = soft.astype(BF)
-        low = (soft - high.astype(F32)).astype(BF)
-        after = jnp.dot(high, triangle_ref[...], preferred_element_type=F32)
-        after = after + jnp.dot(low, triangle_ref[...], preferred_element_type=F32)
+        after = jnp.dot(soft.astype(BF), triangle_ref[...], preferred_element_type=F32)
         return jnp.minimum(scores, 0.0) - tail - after, after[:, :1] + soft[:, :1], packed[:, head:]
 
     def values_of(exponent, valued, allowed=None):
@@ -494,23 +496,21 @@
         lax.fori_loop(first, jnp.minimum(last, z) + 1, one, 0)
 
     def gathering(number, pieces):
-        sign = 1 if number in (0, 3) else -1
+        sign = 1 if number % 2 == 0 else -1
 
         def order(slot, part):
-            return slot * 2 + part
+            return part * 16 + slot
 
         return Plane(pieces, order, plane_recv.at[number], plane_send.at[number], here, sign)
 
-    gathers = [
-        gathering(0, rows.at[0]),
-        gathering(1, rows.at[1]),
-        gathering(2, hidden.at[0]),
-        gathering(3, hidden.at[1]),
-    ]
-    rows0, rows1, hidden0, hidden1 = gathers
+    rows_of = [gathering(n, rows.at[n]) for n in range(GROUPS)]
+    hidden_of = [gathering(GROUPS + n, hidden.at[n]) for n in range(GROUPS)]
+    gathers = rows_of + hidden_of
+    half_width = rows.shape[3]
 
     def lay_out(group):
-        ref = arrived.at[pl.ds(0, nz - 1 + group)]
+        lines = 2 * chips
+        ref = arrived.at[pl.ds(0, lines - (group == 0))]
         pltpu.make_async_remote_copy(
             src_ref=ref,
             dst_ref=ref,
@@ -519,50 +519,57 @@
             device_id={"c": 1 - c},
             device_id_type=MESH,
         ).wait_recv()
-        for n in range(nz):
-            half, line = divmod(n, half_z)
-            rows[group, spot * 2 + half, 2 * line : 2 * line + 2, :] = arrived[group * nz + n]
+        for line in range(lines):
+            for half in range(2):
+                rows[group, half * 16 + spot, 2 * line : 2 * line + 2, :] = arrived[
+                    group * lines + line, :, half * half_width : (half + 1) * half_width
+                ]
 
     def expand(group):
         both = jnp.concatenate([gate_ref[traded], up_ref[traded]], axis=1)
         units = gate_ref.shape[2]
 
         def one(n, none):
-            block = rows[group, pl.ds(n * 8, 8)].reshape(128, -1)
-            flat = jnp.dot(block, both, preferred_element_type=F32)
+            first, second = (
+                rows[group, pl.ds(half * 16 + n * 8, 8)].reshape(128, half_width)
+                for half in range(2)
+            )
+            flat = jnp.dot(first, both[:half_width], preferred_element_type=F32)
+            flat = flat + jnp.dot(second, both[half_width:], preferred_element_type=F32)
             gating = jnp.minimum(flat[:, :units], glu_limit)
             linear = jnp.clip(flat[:, units:], -glu_limit, glu_limit)
             value = gating * jax.nn.sigmoid(glu_alpha * gating) * (linear + 1.0)
-            where = pl.multiple_of(lax.rem(n, 2) * 128, 128)
-            hidden[group, spot * 2 + n // 2, pl.ds(where, 128), :] = value.astype(BF)
+            hidden[group, n * 16 + spot] = value.astype(BF)
             return none
 
-        lax.fori_loop(0, 4, one, 0)
+        lax.fori_loop(0, 2, one, 0)
 
     def contract(group):
-        total = 512
-        results = []
-        for half in range(2):
-            result = jnp.zeros((256, 128), F32)
-            for pair in range(8):
-                units = jnp.concatenate(
-                    [hidden[group, 4 * pair + half], hidden[group, 4 * pair + 2 + half]], axis=1
-                )
-                result = result + jnp.dot(
-                    units, down_ref[traded, pair * 256 : (pair + 1) * 256], preferred_element_type=F32
-                )
-            results.append(result.astype(BF))
-        stacked = jnp.concatenate(results, axis=0)
+        total = 256
+        result = jnp.zeros((total, 128), F32)
+        for pair in range(8):
+            units = jnp.concatenate(
+                [
+                    jnp.concatenate([hidden[group, n], hidden[group, 16 + n]], axis=0)
+                    for n in (2 * pair, 2 * pair + 1)
+                ],
+                axis=1,
+            )
+            result = result + jnp.dot(
+                units,
+                down_ref[traded, pair * 256 : (pair + 1) * 256],
+                preferred_element_type=F32,
+            )
         to, of = iota((total, total), 0), iota((total, total), 1)
-        source = ((to >> 1) & 15) * 32 + (to >> 5) * 2 + (to & 1)
+        source = ((to >> 1) & 15) * 16 + (to >> 5) * 2 + (to & 1)
         turned = jnp.dot(
-            (source == of).astype(F32).astype(BF), stacked, preferred_element_type=F32
+            (source == of).astype(F32).astype(BF), result.astype(BF), preferred_element_type=F32
         ).astype(BF)
-        leaving[group] = turned.reshape(nz, 32, 128)
+        leaving[group] = turned.reshape(2 * chips, 32, 128)
 
     def send_back(o, k):
-        zt, ct = at_z(o - SHIFT_Z), lax.rem(c + k, 2)
-        group, line = divmod(o, half_z)
+        zt, ct = at_z(OFFSETS[o]), lax.rem(c + k, 2)
+        group, line = divmod(o, chips)
         return pltpu.make_async_remote_copy(
             src_ref=leaving.at[group, line * 2 + ct],
             dst_ref=returned.at[expert_here],
@@ -573,19 +580,17 @@
         )
 
     def give_back(group):
-        for o in order:
-            if o // half_z != group:
-                continue
+        for o in order_of(group):
             for k in range(2):
-                if o == SHIFT_Z and k == 0:
+                if o == OWN and k == 0:
 
                     @pl.when(traded == 1)
                     def _():
-                        send_back(SHIFT_Z, 0).start()
+                        send_back(OWN, 0).start()
 
                     @pl.when(traded == 0)
                     def _():
-                        returned[expert_here] = leaving[0, SHIFT_Z * 2 + c]
+                        returned[expert_here] = leaving[0, OWN * 2 + c]
 
                     continue
                 send_back(o, k).start()
@@ -685,78 +690,98 @@
             bulk(gate_ref, trade_send, trade_recv.at[0]).wait_send()
             bulk(down_ref.at[0], trade_send, trade_recv.at[0]).wait_send()
 
-    send_out(0)
-    trade()
-    project()
-    send_out(1)
-    attend_diagonal()
-    lay_out(0)
-    rows0.stage0a()
-    rows0.stage0b()
-    ring(0)
-    tables()
-    rows0.stage1()
-    rows0.stage2()
-    for name in ("gate", "up", "down", "out"):
-        loads[name].wait()
-    ring(1)
-    lay_out(1)
-    rows1.stage0a()
-    rows1.stage0b()
-    rows0.stage3()
-    rows1.stage1()
-    rows0.stage4()
-    traded_in((0, 1))
-    expand(0)
-    hidden0.stage0a()
-    ring(2)
-    rows1.stage2()
-    hidden0.stage0b()
-    partner(0)
-    attend_own()
-    partner(1)
-    partner(2)
-    attend(1, 2)
-    rows1.stage3()
-    hidden0.stage1()
-    rows1.stage4()
-    expand(1)
-    hidden1.stage0a()
-    ring(3)
-    partner(3)
-    partner(4)
-    attend(3, 4)
-    hidden0.stage2()
-    hidden1.stage0b()
-    hidden0.stage3()
-    hidden1.stage1()
-    ring(4)
-    partner(5)
-    partner(6)
-    attend(5, 6)
-    hidden0.stage4()
-    traded_in((2,))
-    contract(0)
-    give_back(0)
-    partner(7)
-    partner(8)
-    attend(7, 8)
-    hidden1.stage2()
-    for step in range(1, downs + 1):
-        partner(step, -1)
-    attend(9, 11)
-    hidden1.stage3()
-    attend(12, nz - 1)
-    store_heads()
-    send_heads()
-    hidden1.stage4()
-    contract(1)
-    give_back(1)
-    wait_heads()
-    mix()
-    take_back()
-    combine()
-    settle()
+    plan = []
+
+    def due(time, name, work, *arguments):
+        plan.append((time, len(plan), name, work, arguments))
+
+    def load_weights():
+        for name in ("gate", "up", "down", "out"):
+            loads[name].wait()
+
+    def expand_and_go(group):
+        expand(group)
+        hidden_of[group].stage0a()
+
+    def contract_and_go(group):
+        contract(group)
+        give_back(group)
+
+    def lay_out_and_go(group):
+        lay_out(group)
+        rows_of[group].stage0a()
+        rows_of[group].stage0b()
+
+    def partners(distances, sign=1):
+        for distance in distances:
+            partner(distance, sign)
+
+    def pass_heads():
+        store_heads()
+        send_heads()
+
+    def pass_heads_if(finished):
+        pl.when(finished)(pass_heads)
+
+    def attend_if(wanted, first, last):
+        pl.when(wanted)(lambda: attend(first, last))
+
+    due(0.0, "send", send_out, 0)
+    due(0.1, "trade", trade)
+    due(0.2, "send", send_out, 1)
+    due(0.3, "project", project)
+    due(0.4, "send", send_out, 2)
+    due(4.0, "send", send_out, 3)
+    due(0.6, "diagonal", attend_diagonal)
+    due(3.0, "tables", tables)
+    due(1.0, "ring", ring, 0)
+    due(9.0, "weights", load_weights)
+    for group, time in enumerate((5.5, 13.4, 15.0, 19.2)):
+        due(time, f"lay{group}", lay_out_and_go, group)
+        for kind, gather in (("rows", rows_of[group]), ("hidden", hidden_of[group])):
+            tag = f"{kind}{group}"
+            due(time + 3.4, tag + "_1", gather.stage1)
+            due(time + 6.4, tag + "_2", gather.stage2)
+            due(time + 9.2, tag + "_3", gather.stage3)
+            due(time + 9.4, tag + "_4", gather.stage4)
+            due(time + 11.0, tag + "_5", gather.stage5)
+            time = time + 11.8
+            if kind == "rows":
+                if group == 0:
+                    due(time - 0.5, "traded", traded_in, (0, 1))
+                due(time - 0.4, f"expand{group}", expand_and_go, group)
+                due(time - 0.2, f"hidden{group}_0", hidden_of[group].stage0b)
+        if group == 0:
+            due(time - 0.5, "traded", traded_in, (2,))
+        due(time - 0.4, f"contract{group}", contract_and_go, group)
+    due(16.7, "ring", ring, 1)
+    due(18.6, "partners", partners, (0, 1, 2))
+    due(18.7, "attend", attend_own)
+    due(18.8, "attend", attend, 1, 2)
+    due(21.6, "ring", ring, 2)
+    due(23.8, "partners", partners, (3, 4))
+    due(23.9, "attend", attend, 3, 4)
+    due(26.6, "ring", ring, 3)
+    due(28.75, "partners", partners, (5, 6))
+    due(28.76, "attend", attend, 5, 6)
+    due(34.45, "ring", ring, 4)
+    due(38.3, "partners", partners, (7, 8))
+    due(38.31, "attend", attend, 7, 8)
+    due(38.32, "partners", partners, tuple(range(1, downs + 1)), -1)
+    due(38.33, "attend", attend_if, z <= 10, 9, 10)
+    due(42.55, "attend", attend_if, z > 10, 9, 10)
+    due(42.6, "attend", attend, 11, 12)
+    due(42.61, "attend", attend, 13, nz - 1)
+    due(38.34, "heads", pass_heads_if, z <= 10)
+    due(42.62, "heads", pass_heads_if, z > 10)
+    due(80.0, "wait_heads", wait_heads)
+    due(80.1, "mix", mix)
+    due(80.2, "take_back", take_back)
+    due(80.3, "combine", combine)
+    due(80.4, "settle", settle)
+    for _, _, name, work, arguments in sorted(plan, key=lambda entry: entry[:2]):
+        with jax.named_scope(name):
+            work(*arguments)
 
 
 def per_device(
@@ -809,9 +834,9 @@
             v((3, tokens, blocks * cap), BF),
             v((length, length), BF),
             v((blocks, 2, width), BF),
-            v((2, 32, 16, width), BF),
-            v((2, 32, 256, 128), BF),
-            v((2, blocks // 2, 32, 128), BF),
+            v((GROUPS, 32, 16, width // 2), BF),
+            v((GROUPS, 32, 128, 128), BF),
+            v((GROUPS, blocks // GROUPS, 32, 128), BF),
             v((blocks, 32, 128), BF),
             v((blocks, length, 2 * head), BF),
             v((16, length // 2, 2 * head), BF),
@@ -820,10 +845,10 @@
             dma((9,)),
             dma((3,)),
             dma,
-            dma((2,)),
+            dma((GROUPS,)),
             dma,
-            dma((4, 2, 9)),
-            dma((4,)),
+            dma((2 * GROUPS, 2, 9)),
+            dma((2 * GROUPS,)),
             dma((blocks - 1,)),
             dma,
             dma,

time: 84.9 us -> 80.9 us (0.953)
  Pallas kernels: 81.3 us -> 77.9 us
    pallas_call x1, Pallas kernels: 81.3 us -> 77.9 us  [per_device(): pl.pallas_call(main_kernel, out_shape=(jax.ShapeDtypeStruct((length, 128)...]
where the time goes in v5:
time: 80.9 us; the launch traced here: 80.7 us
  Pallas kernels  77.9 us (96%)
  local copies, waits for them, and re-layouts  2.1 us (3%)
    pallas_call x1, Pallas kernels, per_device(): pl.pallas_call(main_kernel, out_shape=(jax.ShapeDtypeStruct((length, 128)...  77.9 us
    unnamed x4, local copies, waits for them, and re-layouts  2.1 us

profile of v5, /device:TPU:1, one launch (start us, length us, event | category | flops | bytes accessed | tf_op | source)
XLA Modules:
  0.0 80.7 jit_solution(11003063194355446795)
XLA Ops:
  0.6 77.9 %main.1 = (bf16[256,128]{1,0:T(8,128)(2,1)}, bf16[128,128]{1,0:T(8,128)(2,1)}) custom-call(bf16[256,2048]{1,0:T(8,128)(2,1)} %rows_hbm.1, f32[1,2048]{1,0:T(1,128)} %bitcast.18, bf16[64,2048]{1,0:T(8,128)(2,1)} %bitcast.14, bf16[64,2048]{1,0:T(8,128)(2,1)} %bitcast.15, bf16[64,2048]{1,0:T(8,128)(2,1)} %bitcast.16, f32[32,1,256]{2,1,0:T(1,128)} %bitcast.17, ...), custom_call_target="tpu_custom_call" | custom-call | tf_op jit(solution)/shard_map/main/pallas_call | solution.py:812
  78.6 0.0 copy-start
  78.6 1.5 %copy.18 = bf16[256,128]{1,0:T(8,128)(2,1)} copy(bf16[256,128]{1,0:T(8,128)(2,1)} %get-tuple-element.4) | data formatting | bytes 131072
  80.0 0.0 copy-done
  80.1 0.6 copy.19
Async XLA Ops:
  78.6 1.5 %copy-start = (bf16[128,128]{1,0:T(8,128)(2,1)S(1)}, bf16[128,128]{1,0:T(8,128)(2,1)}, u32[]{:S(2)}) copy-start(bf16[128,128]{1,0:T(8,128)(2,1)} %get-tuple-element.5) | copy-start | bytes 98308

commit v6 on v5

--- a/solution.py
+++ b/solution.py
@@ -233,6 +233,7 @@
     outgoing_ref,
     combine_ref,
     triangle_ref,
+    turning_ref,
     arrived,
     rows,
     hidden,
@@ -544,6 +545,12 @@
 
         lax.fori_loop(0, 2, one, 0)
 
+    def turning():
+        total = turning_ref.shape[0]
+        to, of = iota((total, total), 0), iota((total, total), 1)
+        source = ((to >> 1) & 15) * 16 + (to >> 5) * 2 + (to & 1)
+        turning_ref[...] = (source == of).astype(F32).astype(BF)
+
     def contract(group):
         total = 256
         result = jnp.zeros((total, 128), F32)
@@ -560,10 +567,8 @@
                 down_ref[traded, pair * 256 : (pair + 1) * 256],
                 preferred_element_type=F32,
             )
-        to, of = iota((total, total), 0), iota((total, total), 1)
-        source = ((to >> 1) & 15) * 16 + (to >> 5) * 2 + (to & 1)
         turned = jnp.dot(
-            (source == of).astype(F32).astype(BF), result.astype(BF), preferred_element_type=F32
+            turning_ref[...], result.astype(BF), preferred_element_type=F32
         ).astype(BF)
         leaving[group] = turned.reshape(2 * chips, 32, 128)
 
@@ -734,6 +739,7 @@
     due(4.0, "send", send_out, 3)
     due(0.6, "diagonal", attend_diagonal)
     due(3.0, "tables", tables)
+    due(3.1, "turning", turning)
     due(1.0, "ring", ring, 0)
     due(9.0, "weights", load_weights)
     for group, time in enumerate((5.5, 13.4, 15.0, 19.2)):
@@ -833,6 +839,7 @@
             v((blocks, 2, width), BF),
             v((3, tokens, blocks * cap), BF),
             v((length, length), BF),
+            v((256, 256), BF),
             v((blocks, 2, width), BF),
             v((GROUPS, 32, 16, width // 2), BF),
             v((GROUPS, 32, 128, 128), BF),

time: 80.9 us -> 80.9 us (level)
  no operation moved by 1% of the time
where the time goes in v6:
time: 80.9 us; the launch traced here: 80.7 us
  Pallas kernels  77.9 us (96%)
  local copies, waits for them, and re-layouts  2.1 us (3%)
    pallas_call x1, Pallas kernels, per_device(): pl.pallas_call(main_kernel, out_shape=(jax.ShapeDtypeStruct((length, 128)...  77.9 us
    unnamed x4, local copies, waits for them, and re-layouts  2.1 us

profile of v6, /device:TPU:1, one launch (start us, length us, event | category | flops | bytes accessed | tf_op | source)
XLA Modules:
  0.0 80.7 jit_solution(14630447556979417878)
XLA Ops:
  0.6 77.9 %main.1 = (bf16[256,128]{1,0:T(8,128)(2,1)}, bf16[128,128]{1,0:T(8,128)(2,1)}) custom-call(bf16[256,2048]{1,0:T(8,128)(2,1)} %rows_hbm.1, f32[1,2048]{1,0:T(1,128)} %bitcast.18, bf16[64,2048]{1,0:T(8,128)(2,1)} %bitcast.14, bf16[64,2048]{1,0:T(8,128)(2,1)} %bitcast.15, bf16[64,2048]{1,0:T(8,128)(2,1)} %bitcast.16, f32[32,1,256]{2,1,0:T(1,128)} %bitcast.17, ...), custom_call_target="tpu_custom_call" | custom-call | tf_op jit(solution)/shard_map/main/pallas_call | solution.py:818
  78.5 0.0 copy-start
  78.6 1.5 %copy.18 = bf16[256,128]{1,0:T(8,128)(2,1)} copy(bf16[256,128]{1,0:T(8,128)(2,1)} %get-tuple-element.4) | data formatting | bytes 131072
  80.0 0.0 copy-done
  80.0 0.6 copy.19
Async XLA Ops:
  78.5 1.5 %copy-start = (bf16[128,128]{1,0:T(8,128)(2,1)S(1)}, bf16[128,128]{1,0:T(8,128)(2,1)}, u32[]{:S(2)}) copy-start(bf16[128,128]{1,0:T(8,128)(2,1)} %get-tuple-element.5) | copy-start | bytes 98308
